TPU v7x, 32 devices: a whole 2x2x4 slice. The times are simulated.
32 devices in a mesh: sp: 4 (over z), fs: 4 (over y, x), tp: 2 (over core).
Axes of the slice: x: 2, y: 2, z: 4, core: 2. Of those that a mesh axis runs over, the one named last changes fastest.
Arguments:
- inputs: bfloat16 [2048, 2048], P(('fs', 'sp'), 'tp'), parts along dimension 0, may hold values from -6 to 6
- norm_gain: float32 [2048], replicated, may hold values from 0.1 to 1.9
- in_ssm: bfloat16 [2048, 1024], P('sp', 'tp'), may hold values from -0.125 to 0.125
- in_query: bfloat16 [2048, 1024], P('sp', 'tp')
- in_key: bfloat16 [2048, 256], P('sp', 'tp')
- in_value: bfloat16 [2048, 256], P('sp', 'tp'), may hold values from -0.125 to 0.125
- decay_rate: float32 [64, 64], P('tp'), as said below
- rotation: float32 [64, 64], P('tp'), may hold values from 0.05 to 3
- input_parts: bfloat16 [2, 64, 64, 16], P(None, 'tp')
- output_parts: bfloat16 [2, 64, 16, 64], P(None, 'tp'), may hold values from -0.5 to 0.5
- skip_scale: float32 [64, 16], P('tp'), may hold values from -4 to 4
- decay_shift: float32 [2048, 64], P(('fs', 'sp'), 'tp'), parts along dimension 0, may hold values from -1 to 0
- sink_logit: float32 [16], P('tp'), may hold values from 2 to 6
- out_state: bfloat16 [1024, 2048], P('tp', 'sp'), may hold values from -0.125 to 0.125
- out_attend: bfloat16 [1024, 2048], P('tp', 'sp'), may hold values from -0.125 to 0.125
Outputs:
- mixed: bfloat16 [2048, 2048], P(('fs', 'sp', 'tp')), parts along dimension 0
There are 4 independent parts, one for each index of `fs`. A program takes and returns all parts, laid end to end along the dimension named above; an argument that names none is the same for every part. Nothing has to cross between parts.
Inputs may be any that keep to these rules, and one draw needn't show every extreme that they name: `decay_rate`: between 1e-5 and 0.1.
All inputs are finite; a program needn't handle non-finite values.
Results may differ from a plain program's by a relative error of at most 0.012.
Values may be sent and summed in bfloat16 or wider, within the bound.
A program may use at most 64 MiB of HBM per device.

v0:
```python
import functools
import jax
import jax.numpy as jnp
from jax import lax
from jax.experimental import pallas as pl
from jax.experimental.pallas import tpu as pltpu
from jax.sharding import PartitionSpec as P

GROUP_CH = 16
HEAD_DIM = 64
WINDOW = 128
BLOCK = 128


epsilon = 1e-06
floor_score = -1e30


def prefix(x, axis, join, neutral):
    place = lax.axis_index(axis)
    gathered = jax.tree.map(
        lambda a, kind: lax.all_gather(a.astype(kind), axis),
        x,
        (jnp.bfloat16, jnp.bfloat16, jnp.bfloat16, jnp.bfloat16),
    )
    state = jax.tree.map(lambda a, e: jnp.zeros_like(a) + jnp.asarray(e, a.dtype), x, neutral)

    def one(hop, state):
        return join(
            state,
            jax.tree.map(
                lambda a, own: lax.dynamic_index_in_dim(a, hop, 0, False).astype(own.dtype),
                gathered,
                x,
            ),
        )

    return lax.fori_loop(0, place, one, state)


def from_behind(value, axis, steps):
    count = lax.axis_size(axis)
    initial, last = (max(0, -steps), min(count, count - steps))
    return lax.ppermute(value, axis, [(source, source + steps) for source in range(initial, last)])


def combine(earlier, later):
    first_re, first_im, state_re, state_im = earlier
    second_re, second_im, input_re, input_im = later
    return (
        second_re * first_re - second_im * first_im,
        second_re * first_im + second_im * first_re,
        second_re * state_re - second_im * state_im + input_re,
        second_re * state_im + second_im * state_re + input_im,
    )


def input_matrix(decay_rate, rotation, input_parts):
    damped = jnp.exp(-decay_rate)
    lift_re = damped * jnp.cos(rotation) - 1.0
    lift_im = damped * jnp.sin(rotation)
    modulus = decay_rate * decay_rate + rotation * rotation
    factor_re = (rotation * lift_im - decay_rate * lift_re) / modulus
    factor_im = -(rotation * lift_re + decay_rate * lift_im) / modulus
    part_re = input_parts[0].astype(jnp.float32)
    part_im = input_parts[1].astype(jnp.float32)
    joined_re = factor_re[:, :, None] * part_re - factor_im[:, :, None] * part_im
    joined_im = factor_re[:, :, None] * part_im + factor_im[:, :, None] * part_re
    return jnp.concatenate([joined_re, joined_im], axis=1).astype(jnp.bfloat16)


def window_attention(queries, keys_win, values_win, starts, sink_logit):
    window = queries.shape[1]
    scores = jnp.einsum("nqgrd,nkgd->ngrqk", queries, keys_win, preferred_element_type=jnp.float32)
    scores = scores * queries.shape[-1] ** (-0.5)
    places = (
        jnp.arange(window, dtype=jnp.int32)[:, None]
        + window
        - jnp.arange(2 * window, dtype=jnp.int32)[None, :]
    )
    inside = (places >= 0) & (places < window)
    reach = starts[:, None] - window + jnp.arange(2 * window, dtype=jnp.int32)[None, :] >= 0
    valid = (inside[None] & reach[:, None, :])[:, None, None]
    sinks = sink_logit.reshape(scores.shape[1], scores.shape[2])[None, :, :, None, None]
    scores = jnp.where(valid, scores, floor_score)
    row_peak = jnp.maximum(jnp.max(scores, axis=-1, keepdims=True), sinks)
    raised = jnp.where(valid, jnp.exp(scores - row_peak), 0.0)
    denominator = jnp.sum(raised, axis=-1, keepdims=True) + jnp.exp(sinks - row_peak)
    weights = (raised / denominator).astype(jnp.bfloat16)
    result = jnp.einsum(
        "ngrqk,nkgd->nqgrd", weights, values_win, preferred_element_type=jnp.float32
    )
    return result.astype(jnp.bfloat16)


def general_body(
    inputs,
    norm_gain,
    in_ssm,
    in_query,
    in_key,
    in_value,
    decay_rate,
    rotation,
    input_parts,
    output_parts,
    skip_scale,
    decay_shift,
    sink_logit,
    out_state,
    out_attend,
):
    gathered = lax.all_gather(inputs, "tp", axis=1, tiled=True)
    length = gathered.shape[0]
    widened = gathered.astype(jnp.float32)
    scale = lax.rsqrt(jnp.mean(widened * widened, axis=1, keepdims=True) + epsilon)
    normed = (widened * scale * norm_gain).astype(jnp.bfloat16)

    def add_rows(pieces):
        return tuple(
            (jnp.dot(normed, piece, preferred_element_type=jnp.float32) for piece in pieces)
        )

    projected = add_rows(
        (
            lax.all_gather(in_ssm, "sp", axis=0, tiled=True),
            lax.all_gather(in_query, "sp", axis=0, tiled=True),
            lax.all_gather(in_key, "sp", axis=0, tiled=True),
            lax.all_gather(in_value, "sp", axis=0, tiled=True),
        )
    )
    drive_in, queries, keys_local, values = [piece.astype(jnp.bfloat16) for piece in projected]
    groups = decay_rate.shape[0]
    state_dim = decay_rate.shape[1]
    channels = groups * GROUP_CH
    highest = lax.Precision.HIGHEST
    drive_cols = jnp.transpose(drive_in).reshape(groups, GROUP_CH, length)
    in_matrix = input_matrix(decay_rate, rotation, input_parts)
    drive = jnp.einsum("gqh,ght->gqt", in_matrix, drive_cols, preferred_element_type=jnp.float32)
    shift_cols = jnp.transpose(decay_shift)
    running = jnp.cumsum(shift_cols, axis=1)
    total_shift = running[:, -1]
    remain = length - 1.0 - jnp.arange(length, dtype=jnp.float32)
    to_end = (total_shift[:, None] - running)[:, None, :] - decay_rate[:, :, None] * remain[
        None, None, :
    ]
    fade = jnp.exp(to_end)
    turn = rotation[:, :, None] * remain[None, None, :]
    weight_re = fade * jnp.cos(turn)
    weight_im = fade * jnp.sin(turn)
    drive_re = drive[:, :state_dim]
    drive_im = drive[:, state_dim:]
    final_re = jnp.sum(weight_re * drive_re - weight_im * drive_im, axis=2)
    final_im = jnp.sum(weight_re * drive_im + weight_im * drive_re, axis=2)
    overall = jnp.exp(total_shift[:, None] - decay_rate * length)
    nothing = jnp.zeros_like(final_re)
    carried = prefix(
        (
            overall * jnp.cos(rotation * length),
            overall * jnp.sin(rotation * length),
            final_re,
            final_im,
        ),
        "sp",
        combine,
        (jnp.ones_like(final_re), nothing, nothing, nothing),
    )
    key_heads = keys_local.shape[1] // HEAD_DIM
    query_heads = queries.shape[1] // HEAD_DIM
    windows_dev = length // WINDOW
    previous = from_behind((keys_local, values), "sp", 1)

    def windows(flat, before):
        split = jnp.concatenate([before, flat], axis=0).reshape(
            windows_dev + 1, WINDOW, key_heads, HEAD_DIM
        )
        return jnp.concatenate([split[:-1], split[1:]], axis=1)

    offset = lax.axis_index("sp") * length
    starts = offset + jnp.arange(windows_dev, dtype=jnp.int32) * WINDOW
    queries_blk = queries.reshape(
        windows_dev, WINDOW, key_heads, query_heads // key_heads, HEAD_DIM
    )
    attended = window_attention(
        queries_blk,
        windows(keys_local, previous[0]),
        windows(values, previous[1]),
        starts,
        sink_logit,
    )
    attend_out = attended.reshape(length, query_heads * HEAD_DIM)
    blocks = length // BLOCK
    triangle = (
        jnp.arange(BLOCK, dtype=jnp.int32)[:, None] <= jnp.arange(BLOCK, dtype=jnp.int32)[None, :]
    ).astype(jnp.float32)
    offsets = jnp.arange(BLOCK, dtype=jnp.float32)
    centre = BLOCK // 2
    read_re = output_parts[0].astype(jnp.float32)
    read_im = output_parts[1].astype(jnp.float32)
    angle = rotation[:, :, None] * (offsets - centre)[None, None, :]
    cos_angle = jnp.cos(angle)
    sin_angle = jnp.sin(angle)
    phase = rotation[:, :, None] * (offsets + 1.0)[None, None, :]
    cos_phase = jnp.cos(phase)
    sin_phase = jnp.sin(phase)

    def advance(carry, pieces):
        carry_re, carry_im = carry
        part_re, part_im, shift_part, grouped_part = pieces
        level = jnp.dot(shift_part, triangle, precision=highest)
        log_from = level[:, None, :] - decay_rate[:, :, None] * (offsets + 1.0)[None, None, :]
        relative = log_from - log_from[:, :, centre : centre + 1]
        shrink = jnp.exp(-relative)
        lift_re = shrink * (part_re * cos_angle + part_im * sin_angle)
        lift_im = shrink * (part_im * cos_angle - part_re * sin_angle)
        prefix_re = jnp.dot(lift_re.reshape(groups * state_dim, BLOCK), triangle, precision=highest)
        prefix_im = jnp.dot(lift_im.reshape(groups * state_dim, BLOCK), triangle, precision=highest)
        prefix_re = prefix_re.reshape(groups, state_dim, BLOCK)
        prefix_im = prefix_im.reshape(groups, state_dim, BLOCK)
        grow = jnp.exp(relative)
        from_start = jnp.exp(log_from)
        keep_re = from_start * cos_phase
        keep_im = from_start * sin_phase
        state_re = grow * (prefix_re * cos_angle - prefix_im * sin_angle)
        state_im = grow * (prefix_im * cos_angle + prefix_re * sin_angle)
        state_re = state_re + keep_re * carry_re[:, :, None] - keep_im * carry_im[:, :, None]
        state_im = state_im + keep_re * carry_im[:, :, None] + keep_im * carry_re[:, :, None]
        result = jnp.einsum("ghp,gpt->ght", read_re, state_re, precision=highest)
        result = result - jnp.einsum("ghp,gpt->ght", read_im, state_im, precision=highest)
        result = result + skip_scale[:, :, None] * grouped_part.astype(jnp.float32)
        return ((state_re[:, :, -1], state_im[:, :, -1]), jax.nn.gelu(result).astype(jnp.bfloat16))

    drive_blocks = jnp.transpose(drive.reshape(groups, 2 * state_dim, blocks, BLOCK), (2, 0, 1, 3))
    shift_blocks = jnp.transpose(shift_cols.reshape(groups, blocks, BLOCK), (1, 0, 2))
    grouped_blocks = jnp.transpose(
        drive_cols.reshape(groups, GROUP_CH, blocks, BLOCK), (2, 0, 1, 3)
    )
    _, state_blocks = lax.scan(
        advance,
        (carried[2], carried[3]),
        (
            drive_blocks[:, :, :state_dim],
            drive_blocks[:, :, state_dim:],
            shift_blocks,
            grouped_blocks,
        ),
    )
    state_out = jnp.transpose(state_blocks, (0, 3, 1, 2)).reshape(length, channels)
    column_state, column_attend = (
        lax.all_gather(out_state, "sp", axis=1, tiled=True),
        lax.all_gather(out_attend, "sp", axis=1, tiled=True),
    )
    result = jnp.dot(state_out, column_state, preferred_element_type=jnp.float32)
    return lax.psum_scatter(
        (result + jnp.dot(attend_out, column_attend, preferred_element_type=jnp.float32)).astype(
            jnp.bfloat16
        ),
        "tp",
        scatter_dimension=0,
        tiled=True,
    )


MESH = pl.DeviceIdType.MESH
ANY = pl.BlockSpec(memory_space=pl.ANY)


def remote(src, dst, send, recv, **where):
    return pltpu.make_async_remote_copy(
        src_ref=src, dst_ref=dst, send_sem=send, recv_sem=recv, device_id=where, device_id_type=MESH
    )


def greet(peers):
    barrier = pltpu.get_barrier_semaphore()
    for peer in peers:
        pl.semaphore_signal(barrier, inc=1, device_id=peer, device_id_type=MESH)
    pl.semaphore_wait(barrier, len(peers))


def spread_kernel(n, n_fs, n_tp, repeat_dev, x, ssm, query, kv, shift, ows, owa,
                  xg, w_ssm, w_query, w_kv, shift_g, ows_g, owa_g,
                  held_x, held_w, held_s, held_o, held_p,
                  x_send, x_recv, q_send, q_recv, xp_send, xp_recv, w_send, w_recv, f_send, f_recv,
                  s_send, s_recv, o_send, o_recv, in_sem, out_sem):
    k = lax.axis_index("sp")
    f = lax.axis_index("fs")
    t = lax.axis_index("tp")
    tokens, half = x.shape
    rows = ssm.shape[0]
    part = rows // n_fs
    cs, cq = w_ssm.shape[1], w_query.shape[1]
    groups = shift_g.shape[0]
    other = 1 - t
    peers = [{"sp": lax.rem(k + s, n)} for s in range(1, n)]
    peers += [{"fs": lax.rem(f + d, n_fs)} for d in range(1, n_fs)]
    peers += [{"tp": other}]
    greet(peers)
    order = sorted(range(1, n), key=lambda s: -min(s, n - s))

    def piece(which, place, span):
        if which == 0:
            return ssm.at[span, pl.ds(pl.multiple_of(place * cs, 128), cs)]
        if which == 1:
            return query.at[span, pl.ds(pl.multiple_of(place * cq, 128), cq)]
        return kv.at[lax.div(place, repeat_dev), span]

    dests = (w_ssm, w_query, w_kv)

    def x_at(j, side):
        return xg.at[pl.ds(pl.multiple_of(j * tokens, 128), tokens),
                     pl.ds(pl.multiple_of(side * half, 128), half)]

    copies = []
    for s in order:
        peer = lax.rem(k + s, n)
        for which in range(3):
            mine = pl.ds(pl.multiple_of(f * part, 16), part)
            into = pl.ds(pl.multiple_of(k * rows + f * part, 16), part)
            copies.append(remote(piece(which, peer, mine), dests[which].at[into],
                                 w_send.at[which, s - 1], w_recv.at[which, s - 1], sp=peer))
            copies[-1].start()
    partner = [remote(x, x_at(k, t), xp_send.at[0], xp_recv.at[0], tp=other)]
    partner[0].start()
    for s in order:
        peer = lax.rem(k + s, n)
        c = remote(shift.at[pl.ds(pl.multiple_of(peer * groups, 8), groups)],
                   shift_g.at[:, pl.ds(pl.multiple_of(k * tokens, 128), tokens)],
                   s_send.at[s - 1], s_recv.at[s - 1], sp=peer)
        c.start()
        copies.append(c)

    def hop(step, way):
        block = lax.rem(k - way * step + n, n)
        dst = x_at(block, t)
        src = x if step == 0 else dst
        to = lax.rem(k + way + n, n)
        i = 0 if way > 0 else 1
        active = jnp.logical_and(k + way >= 0, k + way < n)
        active = jnp.logical_and(active, jnp.logical_and(k - way * step >= 0, k - way * step < n))
        return active, remote(src, dst, x_send.at[i, step], x_recv.at[i, step], sp=to)

    def arrival(step, way):
        origin = k - way * (step + 1)
        block = x_at(lax.rem(origin + n, n), t)
        i = 0 if way > 0 else 1
        active = jnp.logical_and(origin >= 0, origin < n)
        c = remote(block, block, x_send.at[i, step], x_recv.at[i, step], sp=lax.rem(k - way + n, n))
        p = remote(block, block, q_send.at[i, step], q_recv.at[i, step], tp=other)
        return active, c, p

    def start_hops(step):
        for way in (1, -1):
            active, c = hop(step, way)

            @pl.when(active)
            def _():
                c.start()

    start_hops(0)
    o_rows = pl.ds(pl.multiple_of(t * ows.shape[0], 16), ows.shape[0])
    for i, (src, dst) in enumerate(((ows, ows_g), (owa, owa_g))):
        c = remote(src, dst.at[o_rows], o_send.at[i], o_recv.at[i], tp=other)
        c.start()
        copies.append(c)
    everything = pl.ds(0, rows)
    here = pl.ds(pl.multiple_of(k * rows, 16), rows)
    local = [(x, held_x, x_at(k, t))]
    for which in range(3):
        local.append((piece(which, k, everything), held_w.at[which], dests[which].at[here]))
    local.append((shift.at[pl.ds(pl.multiple_of(k * groups, 8), groups)], held_s,
                  shift_g.at[:, pl.ds(pl.multiple_of(k * tokens, 128), tokens)]))
    local.append((ows, held_o, ows_g.at[o_rows]))
    local.append((owa, held_p, owa_g.at[o_rows]))
    ins = [pltpu.make_async_copy(a, b, in_sem.at[i]) for i, (a, b, _) in enumerate(local)]
    outs = [pltpu.make_async_copy(b, c, out_sem.at[i]) for i, (_, b, c) in enumerate(local)]
    for c in ins:
        c.start()
    for a, b in zip(ins, outs):
        a.wait()
        b.start()
    forwards = []
    for i, s in enumerate(sorted(range(1, n), key=lambda s: min(s, n - s))):
        source = lax.rem(k + n - s, n)
        into = pl.ds(pl.multiple_of(source * rows + f * part, 16), part)
        for which in range(3):
            got = dests[which].at[into]
            remote(got, got, w_send.at[which, s - 1], w_recv.at[which, s - 1], sp=source).wait_recv()
            for d in range(1, n_fs):
                c = remote(got, got, f_send.at[which, s - 1, d - 1], f_recv.at[which, s - 1, d - 1],
                           fs=lax.rem(f + d, n_fs))
                c.start()
                forwards.append(c)
    for step in range(n - 1):
        for way in (1, -1):
            active, c, p = arrival(step, way)

            @pl.when(active)
            def _():
                c.wait_recv()
                p.start()

        if step + 1 < n - 1:
            start_hops(step + 1)
    for step in range(n - 1):
        for way in (1, -1):
            active, c = hop(step, way)

            @pl.when(active)
            def _():
                c.wait_send()

            active, _c, p = arrival(step, way)

            @pl.when(active)
            def _():
                p.wait()

    for c in copies:
        c.wait_send()
    for c in copies[3 * (n - 1):]:
        c.wait_recv()
    for c in partner + forwards:
        c.wait()
    for c in outs:
        c.wait()


def spread(n, n_fs, n_tp, repeat_dev, x, ssm, query, kv, shift, ows, owa):
    tokens, half = x.shape
    rows = ssm.shape[0]
    cs, cq, ck = ssm.shape[1] // n, query.shape[1] // n, kv.shape[2]
    groups = shift.shape[0] // n
    bf = jnp.bfloat16
    dma = pltpu.SemaphoreType.DMA
    return pl.pallas_call(
        functools.partial(spread_kernel, n, n_fs, n_tp, repeat_dev),
        out_shape=[
            jax.ShapeDtypeStruct((n * tokens, n_tp * half), bf),
            jax.ShapeDtypeStruct((n * rows, cs), bf),
            jax.ShapeDtypeStruct((n * rows, cq), bf),
            jax.ShapeDtypeStruct((n * rows, ck), bf),
            jax.ShapeDtypeStruct((groups, n * tokens), jnp.float32),
            jax.ShapeDtypeStruct((n_tp * ows.shape[0], ows.shape[1]), bf),
            jax.ShapeDtypeStruct((n_tp * owa.shape[0], owa.shape[1]), bf),
        ],
        in_specs=[ANY] * 7,
        out_specs=[ANY] * 7,
        scratch_shapes=[
            pltpu.VMEM(x.shape, bf),
            pltpu.VMEM((3, rows, cs), bf),
            pltpu.VMEM((groups, tokens), jnp.float32),
            pltpu.VMEM(ows.shape, bf),
            pltpu.VMEM(owa.shape, bf),
            dma((2, n - 1)), dma((2, n - 1)), dma((2, n - 1)), dma((2, n - 1)), dma((1,)), dma((1,)),
            dma((3, n - 1)), dma((3, n - 1)),
            dma((3, n - 1, n_fs - 1)), dma((3, n - 1, n_fs - 1)),
            dma((n - 1,)), dma((n - 1,)), dma((2,)), dma((2,)), dma((7,)), dma((7,)),
        ],
        compiler_params=pltpu.CompilerParams(collective_id=0, has_side_effects=True),
    )(x, ssm, query, kv, shift, ows, owa)


def finish_kernel(n, hs, ha, ows, owa, out, got, passing, mixed,
                  h_send, h_recv, p_send, p_recv, own_send, own_recv, o_send, o_recv, in_sem, out_sem):
    k = lax.axis_index("sp")
    t = lax.axis_index("tp")
    other = 1 - t
    sources = (hs, ha)
    chunks = [(i, r) for r in (1, 0) for i in range(2)]
    greet([{"sp": lax.rem(k + s, n)} for s in range(1, n)] + [{"tp": other}])

    def landing(j, i, r):
        return passing.at[i, j] if r else got.at[i, t * n + j]

    def hop(step, way, chunk):
        i, r = chunks[chunk]
        origin = k - way * step
        dst = landing(lax.rem(origin + n, n), i, r)
        src = dst
        if step == 0:
            src = sources[i].at[other if r else t]
        active = jnp.logical_and(k + way >= 0, k + way < n)
        active = jnp.logical_and(active, jnp.logical_and(origin >= 0, origin < n))
        w = 0 if way > 0 else 1
        return active, remote(src, dst, h_send.at[w, step, chunk], h_recv.at[w, step, chunk],
                              sp=lax.rem(k + way + n, n))

    def arrival(step, way, chunk):
        i, r = chunks[chunk]
        origin = k - way * (step + 1)
        active = jnp.logical_and(origin >= 0, origin < n)
        j = lax.rem(origin + n, n)
        w = 0 if way > 0 else 1
        block = landing(j, i, r)
        c = remote(block, block, h_send.at[w, step, chunk], h_recv.at[w, step, chunk],
                   sp=lax.rem(k - way + n, n))
        p = None
        if r:
            p = remote(block, got.at[i, t * n + j], p_send.at[w, step, i], p_recv.at[w, step, i],
                       tp=other)
        return active, c, p

    for chunk in range(4):
        for way in (1, -1):
            active, c = hop(0, way, chunk)

            @pl.when(active)
            def _():
                c.start()

    own = []
    for i in range(2):
        c = remote(sources[i].at[other], got.at[i, t * n + k], own_send.at[i], own_recv.at[i], tp=other)
        c.start()
        own.append(c)
        c = pltpu.make_async_copy(sources[i].at[t], got.at[i, t * n + k], in_sem.at[i])
        c.start()
        own.append(c)
    for step in range(n - 1):
        for chunk in range(4):
            for way in (1, -1):
                active, c, p = arrival(step, way, chunk)

                @pl.when(active)
                def _():
                    c.wait_recv()
                    if p is not None:
                        p.start()

                if step + 1 < n - 1:
                    further, onward = hop(step + 1, way, chunk)

                    @pl.when(further)
                    def _():
                        onward.start()

    for step in range(n - 1):
        for chunk in range(4):
            for way in (1, -1):
                active, c = hop(step, way, chunk)

                @pl.when(active)
                def _():
                    c.wait_send()

                arrived, _c, p = arrival(step, way, chunk)
                if p is not None:

                    @pl.when(arrived)
                    def _():
                        p.wait()

    for c in own:
        c.wait()
    total = None
    for i, weights in enumerate((ows, owa)):
        rows = jnp.concatenate([got[i, j] for j in range(2 * n)], axis=1)
        term = jnp.dot(rows, weights[...], preferred_element_type=jnp.float32)
        total = term if total is None else total + term
    count, width = mixed.shape[1], mixed.shape[2]
    for j in range(n):
        mixed[j] = total[j * count : (j + 1) * count].astype(mixed.dtype)
    columns = pl.ds(pl.multiple_of(k * width, 128), width)
    copies = []
    for s in sorted(range(1, n), key=lambda s: -min(s, n - s)):
        peer = lax.rem(k + s, n)
        c = remote(mixed.at[peer], out.at[:, columns], o_send.at[s], o_recv.at[s], sp=peer)
        c.start()
        copies.append(c)
    c = pltpu.make_async_copy(mixed.at[k], out.at[:, columns], out_sem.at[0])
    c.start()
    c.wait()
    for c in copies:
        c.wait()


def finish(n, hs, ha, ows, owa):
    _, rows, width = hs.shape
    cols = ows.shape[1]
    dma = pltpu.SemaphoreType.DMA
    vmem = pl.BlockSpec(memory_space=pltpu.VMEM)
    bf = jnp.bfloat16
    return pl.pallas_call(
        functools.partial(finish_kernel, n),
        out_shape=jax.ShapeDtypeStruct((rows // n, n * cols), bf),
        in_specs=[vmem] * 4,
        out_specs=ANY,
        scratch_shapes=[
            pltpu.VMEM((2, 2 * n, rows, width), bf),
            pltpu.VMEM((2, n, rows, width), bf),
            pltpu.VMEM((n, rows // n, cols), bf),
            dma((2, n - 1, 4)), dma((2, n - 1, 4)), dma((2, n - 1, 2)), dma((2, n - 1, 2)),
            dma((2,)), dma((2,)), dma((n,)), dma((n,)), dma((2,)), dma((1,)),
        ],
        compiler_params=pltpu.CompilerParams(collective_id=1, has_side_effects=True),
    )(hs, ha, ows, owa)


def halves(x):
    high = x.astype(jnp.bfloat16)
    return high, (x - high.astype(jnp.float32)).astype(jnp.bfloat16)


def split_dot(x, exact):
    high, low = halves(x)
    return jnp.dot(high, exact, preferred_element_type=jnp.float32) + jnp.dot(
        low, exact, preferred_element_type=jnp.float32
    )


def column(row):
    size = row.shape[1]
    same = lax.broadcasted_iota(jnp.int32, (size, size), 0) == lax.broadcasted_iota(
        jnp.int32, (size, size), 1
    )
    return jnp.sum(jnp.where(same, row, 0.0), axis=1, keepdims=True)


def mixer_kernel(k, x, gain, w_ssm, w_query, w_kv, shift, rate, rotation, in_parts, out_parts,
                 skip, sinks, hs, ha, u_scr, q_scr, kv_scr, y_scr):
    f32, bf = jnp.float32, jnp.bfloat16
    length = x.shape[0]
    blocks = length // BLOCK
    groups = shift.shape[0]
    state = rate.shape[1]
    heads = w_query.shape[1] // HEAD_DIM
    side = BLOCK // 2
    kv_scr[0:WINDOW, :] = jnp.zeros((WINDOW, kv_scr.shape[1]), bf)

    for b in range(blocks):
        span = slice(b * BLOCK, (b + 1) * BLOCK)
        wide = x[span, :].astype(f32)
        scale = lax.rsqrt(jnp.mean(wide * wide, axis=1, keepdims=True) + epsilon)
        normed = (wide * scale * gain[...]).astype(bf)
        u = jnp.dot(normed, w_ssm[...], preferred_element_type=f32)
        u_scr[:, span] = jnp.transpose(u.astype(bf).astype(f32))
        q_scr[span, :] = jnp.dot(normed, w_query[...], preferred_element_type=f32).astype(bf)
        kv_scr[(b + 1) * BLOCK : (b + 2) * BLOCK, :] = jnp.dot(
            normed, w_kv[...], preferred_element_type=f32
        ).astype(bf)

    shape = (BLOCK, BLOCK)
    upto = lax.broadcasted_iota(jnp.int32, shape, 0) <= lax.broadcasted_iota(jnp.int32, shape, 1)
    tri = upto.astype(f32).astype(bf)
    centre = BLOCK // 2
    levels, lifts, grows, starts = [], [], [], []
    for b in range(blocks):
        part = shift[:, b * BLOCK : (b + 1) * BLOCK]
        high, low = halves(part)
        low2 = (part - high.astype(f32) - low.astype(f32)).astype(bf)
        level = (
            jnp.dot(high, tri, preferred_element_type=f32)
            + jnp.dot(low, tri, preferred_element_type=f32)
            + jnp.dot(low2, tri, preferred_element_type=f32)
        )
        middle = level[:, centre : centre + 1]
        lifts.append(jnp.exp(middle - level))
        grows.append(jnp.exp(level - middle))
        starts.append(jnp.exp(middle))
    away = lax.broadcasted_iota(jnp.int32, (state, BLOCK), 1).astype(f32) - float(centre)
    first = k * groups
    for g in range(groups):
        rates = column(rate[pl.ds(first + g, 1), :])
        turns = column(rotation[pl.ds(first + g, 1), :])
        angle = turns * away
        cos, sin = jnp.cos(angle), jnp.sin(angle)
        fade = jnp.exp(-rates * away)
        rise = jnp.exp(rates * away)
        up_re, up_im = rise * cos, -(rise * sin)
        down_re, down_im = fade * cos, fade * sin
        line, turn = rate[pl.ds(first + g, 1), :], rotation[pl.ds(first + g, 1), :]
        damped = jnp.exp(-line)
        lift_re = damped * jnp.cos(turn) - 1.0
        lift_im = damped * jnp.sin(turn)
        modulus = line * line + turn * turn
        factor_re = (turn * lift_im - line * lift_re) / modulus
        factor_im = -(turn * lift_re + line * lift_im) / modulus
        part_re = in_parts[0, g].astype(f32)
        part_im = in_parts[1, g].astype(f32)
        in_matrix = jnp.transpose(
            jnp.concatenate(
                [factor_re * part_re - factor_im * part_im, factor_re * part_im + factor_im * part_re],
                axis=1,
            )
        ).astype(bf)
        read = jnp.concatenate(
            [out_parts[0, first + g].astype(f32), -out_parts[1, first + g].astype(f32)], axis=1
        ).astype(bf)
        reach = jnp.exp(-rates * (centre + 1.0))
        reach_re = reach * jnp.cos(turns * (centre + 1.0))
        reach_im = reach * jnp.sin(turns * (centre + 1.0))
        u = u_scr[g * GROUP_CH : (g + 1) * GROUP_CH, :]
        drive = jnp.dot(in_matrix, u.astype(bf), preferred_element_type=f32)
        lifted = []
        for b in range(blocks):
            span = slice(b * BLOCK, (b + 1) * BLOCK)
            row = lifts[b][g : g + 1, :]
            d_re, d_im = drive[:state, span] * row, drive[state:, span] * row
            lifted += [d_re * up_re - d_im * up_im, d_re * up_im + d_im * up_re]
        prefix = split_dot(jnp.concatenate(lifted, axis=0), tri)
        carry_re = jnp.zeros((state, 1), f32)
        carry_im = carry_re
        chosen = lax.broadcasted_iota(jnp.int32, skip.shape, 1) == first + g
        skips = jnp.sum(jnp.where(chosen, skip[...], 0.0), axis=1, keepdims=True)
        for b in range(blocks):
            span = slice(b * BLOCK, (b + 1) * BLOCK)
            begin = starts[b][g : g + 1, :]
            base_re = begin * (carry_re * reach_re - carry_im * reach_im)
            base_im = begin * (carry_re * reach_im + carry_im * reach_re)
            p_re = prefix[2 * b * state : (2 * b + 1) * state] + base_re
            p_im = prefix[(2 * b + 1) * state : (2 * b + 2) * state] + base_im
            row = grows[b][g : g + 1, :]
            s_re = row * (down_re * p_re - down_im * p_im)
            s_im = row * (down_re * p_im + down_im * p_re)
            carry_re, carry_im = s_re[:, BLOCK - 1 :], s_im[:, BLOCK - 1 :]
            high, low = halves(jnp.concatenate([s_re, s_im], axis=0))
            y = jnp.dot(read, high, preferred_element_type=f32) + jnp.dot(
                read, low, preferred_element_type=f32
            )
            y_scr[g * GROUP_CH : (g + 1) * GROUP_CH, span] = y + skips * u[:, span]

    for b in range(blocks):
        y = y_scr[:, b * BLOCK : (b + 1) * BLOCK]
        y = jnp.transpose(jax.nn.gelu(y)).astype(bf)
        hs[0, b * side : (b + 1) * side, :] = y[:side]
        hs[1, b * side : (b + 1) * side, :] = y[side:]

    wide = (WINDOW, 2 * WINDOW)
    gap = lax.broadcasted_iota(jnp.int32, wide, 0) + WINDOW - lax.broadcasted_iota(jnp.int32, wide, 1)
    inside = (gap >= 0) & (gap < WINDOW)
    inside_first = inside & (lax.broadcasted_iota(jnp.int32, wide, 1) >= WINDOW)
    for b in range(blocks):
        keys = kv_scr[b * WINDOW : (b + 2) * WINDOW, :HEAD_DIM]
        values = kv_scr[b * WINDOW : (b + 2) * WINDOW, HEAD_DIM:]
        valid = inside if b else inside_first
        outs = []
        for h in range(heads):
            query = q_scr[b * WINDOW : (b + 1) * WINDOW, h * HEAD_DIM : (h + 1) * HEAD_DIM]
            scores = lax.dot_general(query, keys, (((1,), (1,)), ((), ())), preferred_element_type=f32)
            scores = jnp.where(valid, scores * HEAD_DIM ** (-0.5), floor_score)
            sink = sinks[k * heads + h]
            peak = jnp.maximum(jnp.max(scores, axis=1, keepdims=True), sink)
            raised = jnp.where(valid, jnp.exp(scores - peak), 0.0)
            total = jnp.sum(raised, axis=1, keepdims=True) + jnp.exp(sink - peak)
            weights = (raised / total).astype(bf)
            outs.append(jnp.dot(weights, values, preferred_element_type=f32))
        out = jnp.concatenate(outs, axis=1).astype(bf)
        ha[0, b * side : (b + 1) * side, :] = out[:side]
        ha[1, b * side : (b + 1) * side, :] = out[side:]


def mixer_entry(*refs):
    mixer_kernel(lax.axis_index("sp"), *refs)


def mixer(x, gain, w_ssm, w_query, w_kv, shift, rate, rotation, in_parts, out_parts, skip, sinks,
          entry=mixer_entry, interpret=False):
    length = x.shape[0]
    vmem = pl.BlockSpec(memory_space=pltpu.VMEM)
    return pl.pallas_call(
        entry,
        out_shape=[
            jax.ShapeDtypeStruct((2, length // 2, w_ssm.shape[1]), jnp.bfloat16),
            jax.ShapeDtypeStruct((2, length // 2, w_query.shape[1]), jnp.bfloat16),
        ],
        in_specs=[vmem] * 11 + [pl.BlockSpec(memory_space=pltpu.SMEM)],
        out_specs=[vmem] * 2,
        scratch_shapes=[
            pltpu.VMEM((w_ssm.shape[1], length), jnp.float32),
            pltpu.VMEM((length, w_query.shape[1]), jnp.bfloat16),
            pltpu.VMEM((length + WINDOW, w_kv.shape[1]), jnp.bfloat16),
            pltpu.VMEM((w_ssm.shape[1], length), jnp.float32),
        ],
        interpret=interpret,
    )(x, gain, w_ssm, w_query, w_kv, shift, rate, rotation, in_parts, out_parts, skip, sinks)


def fast_body(
    inputs, norm_gain, in_ssm, in_query, in_key, in_value, decay_rate, rotation, input_parts,
    output_parts, skip_scale, decay_shift, sink_logit, out_state, out_attend,
):
    n, n_fs, n_tp = lax.axis_size("sp"), lax.axis_size("fs"), lax.axis_size("tp")
    key_heads = in_key.shape[1] // HEAD_DIM
    kv = jnp.stack(
        [
            jnp.concatenate([array[:, h * HEAD_DIM : (h + 1) * HEAD_DIM] for array in (in_key, in_value)], axis=1)
            for h in range(key_heads)
        ]
    )
    gathered, w_ssm, w_query, w_kv, shift_cols, ows, owa = spread(
        n, n_fs, n_tp, n // key_heads, inputs, in_ssm, in_query, kv,
        jnp.transpose(decay_shift), out_state, out_attend,
    )

    def own(array):
        size = array.shape[1] // n
        return lax.dynamic_slice_in_dim(array, lax.axis_index("sp") * size, size, 1)

    by_side_state, by_side_attend = mixer(
        gathered, norm_gain[None], w_ssm, w_query, w_kv, shift_cols, decay_rate, rotation,
        own(jnp.swapaxes(input_parts, 2, 3)), output_parts, skip_scale.T, sink_logit,
    )
    return finish(n, by_side_state, by_side_attend, ows, owa)


def body(*args):
    n, n_fs, n_tp = lax.axis_size("sp"), lax.axis_size("fs"), lax.axis_size("tp")
    inputs, in_ssm, in_query, in_key, decay_rate = args[0], args[2], args[3], args[4], args[6]
    key_heads = in_key.shape[1] // HEAD_DIM
    query_heads = in_query.shape[1] // HEAD_DIM
    fits = (
        n_tp == 2
        and 1 < n <= 8
        and n_fs > 1
        and n % key_heads == 0
        and query_heads % n == 0
        and in_ssm.shape[1] == in_query.shape[1]
        and in_ssm.shape[1] % (128 * n) == 0
        and 2 * HEAD_DIM == in_ssm.shape[1] // n
        and decay_rate.shape[0] % (8 * n) == 0
        and decay_rate.shape[0] * GROUP_CH == in_ssm.shape[1]
        and inputs.shape[0] == BLOCK == WINDOW
        and inputs.shape[1] % 128 == 0
        and in_ssm.shape[0] % (16 * n_fs) == 0
        and args[13].shape[1] % 128 == 0
    )
    return (fast_body if fits else general_body)(*args)


def solution(mesh):
    return jax.shard_map(
        body,
        mesh=mesh,
        in_specs=(
            P(("fs", "sp"), "tp"),
            P(),
            P("sp", "tp"),
            P("sp", "tp"),
            P("sp", "tp"),
            P("sp", "tp"),
            P("tp", None),
            P("tp", None),
            P(None, "tp", None, None),
            P(None, "tp", None, None),
            P("tp", None),
            P(("fs", "sp"), "tp"),
            P("tp"),
            P("tp", "sp"),
            P("tp", "sp"),
        ),
        out_specs=P(("fs", "sp", "tp"), None),
        check_vma=False,
    )
```

profile of v0, /device:TPU:0, one launch (start us, length us, event | category | flops | bytes accessed | tf_op | source)
XLA Modules:
  0.0 86.5 jit_solution(15790388501440956135)
XLA Ops:
  0.0 0.0 copy-start
  0.0 0.9 %copy-done = bf16[2,32,64,16]{2,3,1,0:T(8,128)(2,1)S(1)} copy-done((bf16[2,32,64,16]{2,3,1,0:T(8,128)(2,1)S(1)}, bf16[2,32,64,16]{2,3,1,0:T(8,128)(2,1)}, u32[]{:S(2)}) %copy-start) | copy-done | bytes 131096
  1.0 0.6 dynamic-slice_bitcast_fusion.refs_8_
  1.6 1.1 %fusion = (bf16[512,64]{1,0:T(8,128)(2,1)S(1)}, bf16[512,64]{1,0:T(8,128)(2,1)S(1)}) fusion(bf16[512,128]{1,0:T(8,128)(2,1)} %param.19), kind=kLoop, calls=%fused_computation.4 | loop fusion | bytes 262144 | tf_op jit(solution)/shard_map/slice | solution.py:787
  2.7 1.1 %fusion.1 = (bf16[512,64]{1,0:T(8,128)(2,1)S(1)}, bf16[512,64]{1,0:T(8,128)(2,1)S(1)}) fusion(bf16[512,128]{1,0:T(8,128)(2,1)} %param.20), kind=kLoop, calls=%fused_computation.5 | loop fusion | bytes 262144 | tf_op jit(solution)/shard_map/slice | solution.py:787
  3.7 0.1 maximum_bitcast_fusion
  3.9 0.7 pad_maximum_fusion.kv
  4.6 36.7 %shard_map.145 = (bf16[512,2048]{1,0:T(8,128)(2,1)}, bf16[2048,128]{1,0:T(8,128)(2,1)}, bf16[2048,128]{1,0:T(8,128)(2,1)}, bf16[2048,128]{1,0:T(8,128)(2,1)}, f3...) custom-call(bf16[128,1024]{1,0:T(8,128)(2,1)} %x.1, bf16[512,512]{1,0:T(8,128)(2,1)} %ssm.1, ...), custom_call_target="tpu_custom_call" | custom-call | tf_op jit(solution)/shard_map/pallas_call | solution.py:436
  41.4 14.0 %shard_map.146 = (bf16[2,256,128]{2,1,0:T(8,128)(2,1)}, bf16[2,256,128]{2,1,0:T(8,128)(2,1)}) custom-call(bf16[512,2048]{1,0:T(8,128)(2,1)} %get-tuple-element.14.refs_0_, f32[1,2048]{1,0:T(1,128)} %bitcast.10, bf16[2048,128]{1,0:T(8,128)(2,1)} %get-tuple-element.15.refs_2_, bf16[2048,128]{1,0:T(8,128)(2,1)} %get-tuple-element.16.refs_3_, ...), custom_call_target="tpu_custom_call" | custom-call | tf_op jit(solution)/shard_map/pallas_call | solution.py:761
  55.4 29.4 %shard_map.147 = bf16[64,2048]{1,0:T(8,128)(2,1)} custom-call(bf16[2,256,128]{2,1,0:T(8,128)(2,1)} %get-tuple-element.19.hs, bf16[2,256,128]{2,1,0:T(8,128)(2,1)} %get-tuple-element.20.ha, bf16[1024,512]{1,0:T(8,128)(2,1)} %get-tuple-element.21.ows, bf16[1024,512]{1,0:T(8,128)(2,1)} %get-tuple-element.22.owa), custom_call_target="tpu_custom_call" | custom-call | tf_op jit(solution)/shard_map/pallas_call | solution.py:584
  84.8 1.7 %copy.17 = bf16[64,2048]{1,0:T(8,128)(2,1)} copy(bf16[64,2048]{1,0:T(8,128)(2,1)} %shard_map.147) | data formatting | bytes 524288
Async XLA Ops:
  0.0 1.0 %copy-start = (bf16[2,32,64,16]{2,3,1,0:T(8,128)(2,1)S(1)}, bf16[2,32,64,16]{2,3,1,0:T(8,128)(2,1)}, u32[]{:S(2)}) copy-start(bf16[2,32,64,16]{2,3,1,0:T(8,128)(2,1)} %param.23) | copy-start | bytes 393220
where the time goes:
time: 86.8 us; the launch traced here: 86.5 us
  Pallas kernels  80.2 us (92%)
  local copies, waits for them, and re-layouts  5.4 us (6%)
  other arithmetic  0.88 us (1%)
    pallas_call x1, Pallas kernels, spread(): pl.pallas_call(functools.partial(spread_kernel, n, n_fs, n_tp, repeat_dev...  36.7 us
    pallas_call x1, Pallas kernels, finish(): pl.pallas_call(functools.partial(finish_kernel, n), out_shape=jax.ShapeDt...  29.4 us
    pallas_call x1, Pallas kernels, mixer(): pl.pallas_call(entry, out_shape=[jax.ShapeDtypeStruct((2, length // 2, w_...  14 us
    unnamed x3, local copies, waits for them, and re-layouts  2.62 us
    slice x2, local copies, waits for them, and re-layouts, fast_body(): array[:, h * HEAD_DIM:(h + 1) * HEAD_DIM]  2.16 us

commit v1 on v0

v1 whole, which is shorter than its diff:
```python
import functools
import jax
import jax.numpy as jnp
from jax import lax
from jax.experimental import pallas as pl
from jax.experimental.pallas import tpu as pltpu
from jax.sharding import PartitionSpec as P

GROUP_CH = 16
HEAD_DIM = 64
WINDOW = 128
BLOCK = 128


epsilon = 1e-06
floor_score = -1e30


def prefix(x, axis, join, neutral):
    place = lax.axis_index(axis)
    gathered = jax.tree.map(
        lambda a, kind: lax.all_gather(a.astype(kind), axis),
        x,
        (jnp.bfloat16, jnp.bfloat16, jnp.bfloat16, jnp.bfloat16),
    )
    state = jax.tree.map(lambda a, e: jnp.zeros_like(a) + jnp.asarray(e, a.dtype), x, neutral)

    def one(hop, state):
        return join(
            state,
            jax.tree.map(
                lambda a, own: lax.dynamic_index_in_dim(a, hop, 0, False).astype(own.dtype),
                gathered,
                x,
            ),
        )

    return lax.fori_loop(0, place, one, state)


def from_behind(value, axis, steps):
    count = lax.axis_size(axis)
    initial, last = (max(0, -steps), min(count, count - steps))
    return lax.ppermute(value, axis, [(source, source + steps) for source in range(initial, last)])


def combine(earlier, later):
    first_re, first_im, state_re, state_im = earlier
    second_re, second_im, input_re, input_im = later
    return (
        second_re * first_re - second_im * first_im,
        second_re * first_im + second_im * first_re,
        second_re * state_re - second_im * state_im + input_re,
        second_re * state_im + second_im * state_re + input_im,
    )


def input_matrix(decay_rate, rotation, input_parts):
    damped = jnp.exp(-decay_rate)
    lift_re = damped * jnp.cos(rotation) - 1.0
    lift_im = damped * jnp.sin(rotation)
    modulus = decay_rate * decay_rate + rotation * rotation
    factor_re = (rotation * lift_im - decay_rate * lift_re) / modulus
    factor_im = -(rotation * lift_re + decay_rate * lift_im) / modulus
    part_re = input_parts[0].astype(jnp.float32)
    part_im = input_parts[1].astype(jnp.float32)
    joined_re = factor_re[:, :, None] * part_re - factor_im[:, :, None] * part_im
    joined_im = factor_re[:, :, None] * part_im + factor_im[:, :, None] * part_re
    return jnp.concatenate([joined_re, joined_im], axis=1).astype(jnp.bfloat16)


def window_attention(queries, keys_win, values_win, starts, sink_logit):
    window = queries.shape[1]
    scores = jnp.einsum("nqgrd,nkgd->ngrqk", queries, keys_win, preferred_element_type=jnp.float32)
    scores = scores * queries.shape[-1] ** (-0.5)
    places = (
        jnp.arange(window, dtype=jnp.int32)[:, None]
        + window
        - jnp.arange(2 * window, dtype=jnp.int32)[None, :]
    )
    inside = (places >= 0) & (places < window)
    reach = starts[:, None] - window + jnp.arange(2 * window, dtype=jnp.int32)[None, :] >= 0
    valid = (inside[None] & reach[:, None, :])[:, None, None]
    sinks = sink_logit.reshape(scores.shape[1], scores.shape[2])[None, :, :, None, None]
    scores = jnp.where(valid, scores, floor_score)
    row_peak = jnp.maximum(jnp.max(scores, axis=-1, keepdims=True), sinks)
    raised = jnp.where(valid, jnp.exp(scores - row_peak), 0.0)
    denominator = jnp.sum(raised, axis=-1, keepdims=True) + jnp.exp(sinks - row_peak)
    weights = (raised / denominator).astype(jnp.bfloat16)
    result = jnp.einsum(
        "ngrqk,nkgd->nqgrd", weights, values_win, preferred_element_type=jnp.float32
    )
    return result.astype(jnp.bfloat16)


def general_body(
    inputs,
    norm_gain,
    in_ssm,
    in_query,
    in_key,
    in_value,
    decay_rate,
    rotation,
    input_parts,
    output_parts,
    skip_scale,
    decay_shift,
    sink_logit,
    out_state,
    out_attend,
):
    gathered = lax.all_gather(inputs, "tp", axis=1, tiled=True)
    length = gathered.shape[0]
    widened = gathered.astype(jnp.float32)
    scale = lax.rsqrt(jnp.mean(widened * widened, axis=1, keepdims=True) + epsilon)
    normed = (widened * scale * norm_gain).astype(jnp.bfloat16)

    def add_rows(pieces):
        return tuple(
            (jnp.dot(normed, piece, preferred_element_type=jnp.float32) for piece in pieces)
        )

    projected = add_rows(
        (
            lax.all_gather(in_ssm, "sp", axis=0, tiled=True),
            lax.all_gather(in_query, "sp", axis=0, tiled=True),
            lax.all_gather(in_key, "sp", axis=0, tiled=True),
            lax.all_gather(in_value, "sp", axis=0, tiled=True),
        )
    )
    drive_in, queries, keys_local, values = [piece.astype(jnp.bfloat16) for piece in projected]
    groups = decay_rate.shape[0]
    state_dim = decay_rate.shape[1]
    channels = groups * GROUP_CH
    highest = lax.Precision.HIGHEST
    drive_cols = jnp.transpose(drive_in).reshape(groups, GROUP_CH, length)
    in_matrix = input_matrix(decay_rate, rotation, input_parts)
    drive = jnp.einsum("gqh,ght->gqt", in_matrix, drive_cols, preferred_element_type=jnp.float32)
    shift_cols = jnp.transpose(decay_shift)
    running = jnp.cumsum(shift_cols, axis=1)
    total_shift = running[:, -1]
    remain = length - 1.0 - jnp.arange(length, dtype=jnp.float32)
    to_end = (total_shift[:, None] - running)[:, None, :] - decay_rate[:, :, None] * remain[
        None, None, :
    ]
    fade = jnp.exp(to_end)
    turn = rotation[:, :, None] * remain[None, None, :]
    weight_re = fade * jnp.cos(turn)
    weight_im = fade * jnp.sin(turn)
    drive_re = drive[:, :state_dim]
    drive_im = drive[:, state_dim:]
    final_re = jnp.sum(weight_re * drive_re - weight_im * drive_im, axis=2)
    final_im = jnp.sum(weight_re * drive_im + weight_im * drive_re, axis=2)
    overall = jnp.exp(total_shift[:, None] - decay_rate * length)
    nothing = jnp.zeros_like(final_re)
    carried = prefix(
        (
            overall * jnp.cos(rotation * length),
            overall * jnp.sin(rotation * length),
            final_re,
            final_im,
        ),
        "sp",
        combine,
        (jnp.ones_like(final_re), nothing, nothing, nothing),
    )
    key_heads = keys_local.shape[1] // HEAD_DIM
    query_heads = queries.shape[1] // HEAD_DIM
    windows_dev = length // WINDOW
    previous = from_behind((keys_local, values), "sp", 1)

    def windows(flat, before):
        split = jnp.concatenate([before, flat], axis=0).reshape(
            windows_dev + 1, WINDOW, key_heads, HEAD_DIM
        )
        return jnp.concatenate([split[:-1], split[1:]], axis=1)

    offset = lax.axis_index("sp") * length
    starts = offset + jnp.arange(windows_dev, dtype=jnp.int32) * WINDOW
    queries_blk = queries.reshape(
        windows_dev, WINDOW, key_heads, query_heads // key_heads, HEAD_DIM
    )
    attended = window_attention(
        queries_blk,
        windows(keys_local, previous[0]),
        windows(values, previous[1]),
        starts,
        sink_logit,
    )
    attend_out = attended.reshape(length, query_heads * HEAD_DIM)
    blocks = length // BLOCK
    triangle = (
        jnp.arange(BLOCK, dtype=jnp.int32)[:, None] <= jnp.arange(BLOCK, dtype=jnp.int32)[None, :]
    ).astype(jnp.float32)
    offsets = jnp.arange(BLOCK, dtype=jnp.float32)
    centre = BLOCK // 2
    read_re = output_parts[0].astype(jnp.float32)
    read_im = output_parts[1].astype(jnp.float32)
    angle = rotation[:, :, None] * (offsets - centre)[None, None, :]
    cos_angle = jnp.cos(angle)
    sin_angle = jnp.sin(angle)
    phase = rotation[:, :, None] * (offsets + 1.0)[None, None, :]
    cos_phase = jnp.cos(phase)
    sin_phase = jnp.sin(phase)

    def advance(carry, pieces):
        carry_re, carry_im = carry
        part_re, part_im, shift_part, grouped_part = pieces
        level = jnp.dot(shift_part, triangle, precision=highest)
        log_from = level[:, None, :] - decay_rate[:, :, None] * (offsets + 1.0)[None, None, :]
        relative = log_from - log_from[:, :, centre : centre + 1]
        shrink = jnp.exp(-relative)
        lift_re = shrink * (part_re * cos_angle + part_im * sin_angle)
        lift_im = shrink * (part_im * cos_angle - part_re * sin_angle)
        prefix_re = jnp.dot(lift_re.reshape(groups * state_dim, BLOCK), triangle, precision=highest)
        prefix_im = jnp.dot(lift_im.reshape(groups * state_dim, BLOCK), triangle, precision=highest)
        prefix_re = prefix_re.reshape(groups, state_dim, BLOCK)
        prefix_im = prefix_im.reshape(groups, state_dim, BLOCK)
        grow = jnp.exp(relative)
        from_start = jnp.exp(log_from)
        keep_re = from_start * cos_phase
        keep_im = from_start * sin_phase
        state_re = grow * (prefix_re * cos_angle - prefix_im * sin_angle)
        state_im = grow * (prefix_im * cos_angle + prefix_re * sin_angle)
        state_re = state_re + keep_re * carry_re[:, :, None] - keep_im * carry_im[:, :, None]
        state_im = state_im + keep_re * carry_im[:, :, None] + keep_im * carry_re[:, :, None]
        result = jnp.einsum("ghp,gpt->ght", read_re, state_re, precision=highest)
        result = result - jnp.einsum("ghp,gpt->ght", read_im, state_im, precision=highest)
        result = result + skip_scale[:, :, None] * grouped_part.astype(jnp.float32)
        return ((state_re[:, :, -1], state_im[:, :, -1]), jax.nn.gelu(result).astype(jnp.bfloat16))

    drive_blocks = jnp.transpose(drive.reshape(groups, 2 * state_dim, blocks, BLOCK), (2, 0, 1, 3))
    shift_blocks = jnp.transpose(shift_cols.reshape(groups, blocks, BLOCK), (1, 0, 2))
    grouped_blocks = jnp.transpose(
        drive_cols.reshape(groups, GROUP_CH, blocks, BLOCK), (2, 0, 1, 3)
    )
    _, state_blocks = lax.scan(
        advance,
        (carried[2], carried[3]),
        (
            drive_blocks[:, :, :state_dim],
            drive_blocks[:, :, state_dim:],
            shift_blocks,
            grouped_blocks,
        ),
    )
    state_out = jnp.transpose(state_blocks, (0, 3, 1, 2)).reshape(length, channels)
    column_state, column_attend = (
        lax.all_gather(out_state, "sp", axis=1, tiled=True),
        lax.all_gather(out_attend, "sp", axis=1, tiled=True),
    )
    result = jnp.dot(state_out, column_state, preferred_element_type=jnp.float32)
    return lax.psum_scatter(
        (result + jnp.dot(attend_out, column_attend, preferred_element_type=jnp.float32)).astype(
            jnp.bfloat16
        ),
        "tp",
        scatter_dimension=0,
        tiled=True,
    )


MESH = pl.DeviceIdType.MESH
ANY = pl.BlockSpec(memory_space=pl.ANY)


def remote(src, dst, send, recv, **where):
    return pltpu.make_async_remote_copy(
        src_ref=src, dst_ref=dst, send_sem=send, recv_sem=recv, device_id=where, device_id_type=MESH
    )


def greet(peers):
    barrier = pltpu.get_barrier_semaphore()
    for peer in peers:
        pl.semaphore_signal(barrier, inc=1, device_id=peer, device_id_type=MESH)
    pl.semaphore_wait(barrier, len(peers))


def halves(x):
    high = x.astype(jnp.bfloat16)
    return high, (x - high.astype(jnp.float32)).astype(jnp.bfloat16)


def split_dot(x, exact):
    high, low = halves(x)
    return jnp.dot(high, exact, preferred_element_type=jnp.float32) + jnp.dot(
        low, exact, preferred_element_type=jnp.float32
    )


def column(row):
    size = row.shape[1]
    same = lax.broadcasted_iota(jnp.int32, (size, size), 0) == lax.broadcasted_iota(
        jnp.int32, (size, size), 1
    )
    return jnp.sum(jnp.where(same, row, 0.0), axis=1, keepdims=True)


def layer_kernel(x_in, gain_in, ssm, query, key_in, value_in, rate_in, turn_in, parts_in, reads_in,
                 skip_in, shift_in, sinks_in, ows, owa, out,
                 xf, normed, w_ssm, w_query, w_kv, wo_s, wo_a, key, value, pairs, gain, rate, turn,
                 parts, reads, skip, shift, sinks, tab, inm, read, lifts, grows, prefix, u_scr, q_scr,
                 kv_scr, y_scr, act_s, act_a, carry_out, carry_in, pf, pb, got, fsend, fgot, res,
                 loc, z_s, z_r, p_s, p_r, ax_s, ax_r, ay_s, ay_r, bx_s, bx_r, by_s, by_r,
                 d_s, d_r, e_s, e_r, o_s):
    f32, bf = jnp.float32, jnp.bfloat16
    k, f, t = lax.axis_index("sp"), lax.axis_index("fs"), lax.axis_index("tp")
    n, n_fs = 4, 4
    tokens, half = x_in.shape
    rows, cols = ssm.shape[0], ows.shape[1]
    wide = w_ssm.shape[1]
    groups, state = tab.shape[0], tab.shape[2]
    heads = w_query.shape[1] // HEAD_DIM
    par, late = lax.rem(k, 2), lax.div(k, 2)
    pair = k + 1 - 2 * par
    order = (pair, 2 - late, 3 - 3 * late)
    other = 1 - t
    fx, fy = f + 1 - 2 * lax.rem(f, 2), lax.rem(f + 2, n_fs)
    greet([{"sp": j} for j in order] + [{"fs": fx}, {"fs": fy}, {"tp": other}])

    part, height = rows // n_fs, wide // n_fs
    into = (w_ssm, w_query, w_kv, wo_s, wo_a)

    def region(w, j, q, side=None):
        size = part if w < 3 else height
        first = q * size
        if side is not None:
            size //= 2
            first = first + side * size
        if w < 3:
            return into[w].at[pl.ds(pl.multiple_of(j * rows + first, 16), size)]
        return into[w].at[pl.ds(pl.multiple_of(first, 16), size), pl.ds(pl.multiple_of(j * cols, 128), cols)]

    def piece(w, peer):
        kind = lax.rem(peer, 2)
        mine = pl.ds(pl.multiple_of(f * part, 16), part)
        if w == 2:
            return pairs.at[kind, mine]
        if w < 2:
            return (ssm, query)[w].at[mine, pl.ds(pl.multiple_of(kind * wide, 128), wide)]
        return (ows, owa)[w - 3].at[pl.ds(pl.multiple_of(kind * wide + f * height, 16), height)]

    sent = []

    def launch(c):
        c.start()
        sent.append(c)

    def over_z(w, peer):
        launch(remote(piece(w, peer), region(w, k, f), z_s.at[w, peer], z_r.at[w, k], sp=peer))

    def x_at(e, side):
        return xf.at[pl.ds(pl.multiple_of(e * tokens, 128), tokens), pl.ds(pl.multiple_of(side * half, 128), half)]

    def shift_at(e):
        return shift.at[:, pl.ds(pl.multiple_of(e * tokens, 128), tokens)]

    def shift_rows(e):
        return shift_in.at[pl.ds(pl.multiple_of(e * groups, 8), groups)]

    def z_here(w, j):
        block = region(w, j, f)
        remote(block, block, z_s.at[w, j], z_r.at[w, j], sp=j).wait_recv()
        for side in (0, 1):
            a = region(w, j, f, side)
            launch(remote(a, a, ax_s.at[w, j, side], ax_r.at[w, j, side], fs=fx))
            b = region(w, j, f, 1 - side)
            launch(remote(b, b, ay_s.at[w, j, 1 - side], ay_r.at[w, j, 1 - side], fs=fy))

    def relay(w, j):
        a = region(w, j, fx, 0)
        remote(a, a, ax_s.at[w, j, 0], ax_r.at[w, j, 0], fs=fx).wait_recv()
        launch(remote(a, a, by_s.at[w, j], by_r.at[w, j], fs=fy))
        b = region(w, j, fy, 1)
        remote(b, b, ay_s.at[w, j, 1], ay_r.at[w, j, 1], fs=fy).wait_recv()
        launch(remote(b, b, bx_s.at[w, j], bx_r.at[w, j], fs=fx))

    def complete(w, j):
        a = region(w, j, fx, 1)
        remote(a, a, ax_s.at[w, j, 1], ax_r.at[w, j, 1], fs=fx).wait_recv()
        b = region(w, j, fy, 0)
        remote(b, b, ay_s.at[w, j, 0], ay_r.at[w, j, 0], fs=fy).wait_recv()
        far = n_fs - 1 - f
        a = region(w, j, far, 0)
        remote(a, a, by_s.at[w, j], by_r.at[w, j], fs=fy).wait_recv()
        b = region(w, j, far, 1)
        remote(b, b, bx_s.at[w, j], bx_r.at[w, j], fs=fx).wait_recv()

    def steps_of(ws):
        steps = []
        waiting = []
        for j in order:
            for w in ws:
                steps.append(functools.partial(z_here, w, j))
                if waiting:
                    steps.append(waiting.pop(0))
                waiting.append(functools.partial(relay, w, j))
        return steps + waiting

    queue = steps_of((0,))

    def pump(count):
        for _ in range(count):
            if queue:
                queue.pop(0)()

    for peer in order:
        over_z(0, peer)
    launch(remote(x_in, x_at(par, t), p_s.at[0], p_r.at[0], sp=pair))
    launch(remote(x_in, x_at(par, t), p_s.at[2], p_r.at[2], tp=other))
    launch(remote(shift_rows(1 - par), shift_at(par), p_s.at[1], p_r.at[1], sp=pair))
    for peer in order:
        over_z(1, peer)
    everything = pl.ds(0, rows)
    here = pl.ds(pl.multiple_of(k * rows, 16), rows)
    mine = pl.ds(pl.multiple_of(par * wide, 128), wide)
    columns = pl.ds(pl.multiple_of(k * cols, 128), cols)
    local = [
        (key_in, key), (value_in, value), (rate_in, rate), (turn_in, turn), (parts_in, parts),
        (reads_in, reads), (skip_in, skip), (gain_in, gain), (sinks_in, sinks),
        (shift_rows(par), shift_at(par)), (x_in, x_at(par, t)),
        (ssm.at[everything, mine], w_ssm.at[here]), (query.at[everything, mine], w_query.at[here]),
        (ows.at[mine], wo_s.at[:, columns]), (owa.at[mine], wo_a.at[:, columns]),
    ]
    local = [pltpu.make_async_copy(a, b, loc.at[i]) for i, (a, b) in enumerate(local)]
    for c in local:
        c.start()
    local[0].wait()
    local[1].wait()
    for e in range(2):
        span = slice(e * HEAD_DIM, (e + 1) * HEAD_DIM)
        pairs[e] = jnp.concatenate([key[:, span], value[:, span]], axis=1)
    w_kv[here, :] = pairs[par]
    for c in local[2:11]:
        c.wait()
    first = par * groups

    def tables(g, columns_of):
        line, spin = rate[pl.ds(first + g, 1), :], turn[pl.ds(first + g, 1), :]
        rates, turns = column(line), column(spin)
        away = lax.broadcasted_iota(jnp.int32, (state, BLOCK), 1).astype(f32) - float(BLOCK // 2)
        angle = turns * away
        cos, sin = jnp.cos(angle), jnp.sin(angle)
        fade = jnp.exp(-rates * away)
        rise = jnp.exp(rates * away)
        tab[g, 0] = rise * cos
        tab[g, 1] = -(rise * sin)
        tab[g, 2] = fade * cos
        tab[g, 3] = fade * sin
        damped = jnp.exp(-line)
        lift_re = damped * jnp.cos(spin) - 1.0
        lift_im = damped * jnp.sin(spin)
        modulus = line * line + spin * spin
        factor_re = (spin * lift_im - line * lift_re) / modulus
        factor_im = -(spin * lift_re + line * lift_im) / modulus
        part_re = parts[0, first + g].astype(f32)
        part_im = parts[1, first + g].astype(f32)
        inm[g] = jnp.transpose(
            jnp.concatenate(
                [factor_re * part_re - factor_im * part_im, factor_re * part_im + factor_im * part_re],
                axis=1,
            )
        ).astype(bf)
        read[g] = jnp.concatenate(
            [reads[0, first + g].astype(f32), -reads[1, first + g].astype(f32)], axis=1
        ).astype(bf)
        spot = lax.broadcasted_iota(jnp.int32, (state, BLOCK), 1) == g
        return jnp.where(spot, rates, columns_of[0]), jnp.where(spot, turns, columns_of[1])

    columns_of = (jnp.zeros((state, BLOCK), f32), jnp.zeros((state, BLOCK), f32))
    quarter = groups // 4
    columns_of = lax.fori_loop(0, quarter, tables, columns_of)
    for i, peer in enumerate(order):
        over_z(2, peer)
    for peer in order:
        over_z(3, peer)
        over_z(4, peer)
    pump(2)
    columns_of = lax.fori_loop(quarter, 2 * quarter, tables, columns_of)
    pump(2)

    def normalize(e):
        block = pl.ds(pl.multiple_of(e * tokens, 128), tokens)
        full = xf[block, :].astype(f32)
        scale = lax.rsqrt(jnp.mean(full * full, axis=1, keepdims=True) + epsilon)
        normed[block, :] = (full * scale * gain[...]).astype(bf)

    theirs = x_at(par, other)
    remote(theirs, theirs, p_s.at[2], p_r.at[2], tp=other).wait_recv()
    normalize(par)
    columns_of = lax.fori_loop(2 * quarter, 3 * quarter, tables, columns_of)
    pump(1)
    columns_of = lax.fori_loop(3 * quarter, groups, tables, columns_of)
    pump(len(queue))
    queue += steps_of((1, 2))
    next_x = x_at(1 - par, t)
    remote(next_x, next_x, p_s.at[0], p_r.at[0], sp=pair).wait_recv()
    launch(remote(next_x, next_x, p_s.at[3], p_r.at[3], tp=other))
    near = shift_at(1 - par)
    remote(near, near, p_s.at[1], p_r.at[1], sp=pair).wait_recv()

    shape = (BLOCK, BLOCK)
    upto = lax.broadcasted_iota(jnp.int32, shape, 0) <= lax.broadcasted_iota(jnp.int32, shape, 1)
    tri = upto.astype(f32).astype(bf)
    centre = BLOCK // 2
    eye = lax.broadcasted_iota(jnp.int32, (groups, BLOCK), 0) == lax.broadcasted_iota(
        jnp.int32, (groups, BLOCK), 1
    )

    def across(col):
        return jnp.sum(jnp.where(eye, col, 0.0), axis=0, keepdims=True)

    begins, lasts = [], []
    for b in range(2):
        piece_b = shift[:, b * BLOCK : (b + 1) * BLOCK]
        high, low = halves(piece_b)
        low2 = (piece_b - high.astype(f32) - low.astype(f32)).astype(bf)
        level = (
            jnp.dot(high, tri, preferred_element_type=f32)
            + jnp.dot(low, tri, preferred_element_type=f32)
            + jnp.dot(low2, tri, preferred_element_type=f32)
        )
        middle = level[:, centre : centre + 1]
        lifts[b] = jnp.exp(middle - level)
        grown = jnp.exp(level - middle)
        grows[b] = grown
        begins.append(across(jnp.exp(middle)))
        lasts.append(across(grown[:, BLOCK - 1 :]))
    rates, turns = columns_of

    def times(a, b):
        return a[0] * b[0] - a[1] * b[1], a[0] * b[1] + a[1] * b[0]

    def plus(a, b):
        return a[0] + b[0], a[1] + b[1]

    def scaled(row, a):
        return row * a[0], row * a[1]

    def spiral(count):
        fade = jnp.exp(-rates * count)
        return fade * jnp.cos(turns * count), fade * jnp.sin(turns * count)

    reach, end = spiral(centre + 1.0), spiral(BLOCK - 1.0 - centre)
    whole = times(reach, end)

    theirs = x_at(1 - par, other)
    remote(theirs, theirs, p_s.at[3], p_r.at[3], tp=other).wait_recv()
    normalize(1 - par)
    local[11].wait()
    for j in order:
        complete(0, j)
    u = jnp.dot(normed[...], w_ssm[...], preferred_element_type=f32)
    u_scr[...] = jnp.transpose(u.astype(bf).astype(f32))

    lane = lax.broadcasted_iota(jnp.int32, (state, BLOCK), 1)
    ends = [jnp.zeros((state, BLOCK), f32)] * 4
    for g in range(groups):
        u = u_scr[g * GROUP_CH : (g + 1) * GROUP_CH, :]
        drive = jnp.dot(inm[g], u.astype(bf), preferred_element_type=f32)
        up_re, up_im = tab[g, 0], tab[g, 1]
        lifted = []
        for b in range(2):
            span = slice(b * BLOCK, (b + 1) * BLOCK)
            row = lifts[b, g : g + 1, :]
            d_re, d_im = drive[:state, span] * row, drive[state:, span] * row
            lifted += [d_re * up_re - d_im * up_im, d_re * up_im + d_im * up_re]
        sums = split_dot(jnp.concatenate(lifted, axis=0), tri)
        prefix[g] = sums
        ends = [
            jnp.where(lane == g, sums[i * state : (i + 1) * state, BLOCK - 1 :], ends[i])
            for i in range(4)
        ]
        if g % 2 == 1:
            pump(2)
    pump(len(queue))
    queue += steps_of((3, 4))
    own = [scaled(lasts[b], times(end, (ends[2 * b], ends[2 * b + 1]))) for b in range(2)]
    decay = [scaled(lasts[b] * begins[b], whole) for b in range(2)]
    final = plus(own[1], times(decay[1], own[0]))
    carry_out[...] = jnp.transpose(jnp.concatenate(final, axis=0))[:groups]

    local[12].wait()
    for w in (1, 2):
        for j in order:
            complete(w, j)
    kv_scr[WINDOW:, :] = jnp.dot(normed[...], w_kv[...], preferred_element_type=f32).astype(bf)
    q_scr[...] = jnp.dot(normed[...], w_query[...], preferred_element_type=f32).astype(bf)
    ahead, behind = lax.rem(k + 2, n), lax.rem(k + 2, n)
    tail = kv_scr.at[pl.ds(2 * WINDOW, WINDOW)]
    head = kv_scr.at[pl.ds(0, WINDOW)]
    hand_kv = remote(tail, head, p_s.at[4], p_r.at[4], sp=ahead)
    hand_state = remote(carry_out, carry_in, p_s.at[5], p_r.at[5], sp=ahead)

    @pl.when(late == 0)
    def _():
        hand_kv.start()
        hand_state.start()
        kv_scr[:WINDOW, :] = jnp.zeros((WINDOW, kv_scr.shape[1]), bf)
        carry_in[...] = jnp.zeros(carry_in.shape, f32)

    gap_shape = (WINDOW, 2 * WINDOW)
    at = lax.broadcasted_iota(jnp.int32, gap_shape, 1)
    gap = lax.broadcasted_iota(jnp.int32, gap_shape, 0) + WINDOW - at
    inside = (gap >= 0) & (gap < WINDOW)
    inside_first = inside & (at >= WINDOW * (1 - late))
    sink_lane = lax.broadcasted_iota(jnp.int32, sinks.shape, 1)
    for b in (1, 0):
        if b == 0:

            @pl.when(late == 1)
            def _():
                hand_kv.wait_recv()
                hand_state.wait_recv()

        keys = kv_scr[b * WINDOW : (b + 2) * WINDOW, :HEAD_DIM]
        values = kv_scr[b * WINDOW : (b + 2) * WINDOW, HEAD_DIM:]
        valid = inside if b else inside_first
        outs = []
        for h in range(heads):
            q = q_scr[b * WINDOW : (b + 1) * WINDOW, h * HEAD_DIM : (h + 1) * HEAD_DIM]
            scores = lax.dot_general(q, keys, (((1,), (1,)), ((), ())), preferred_element_type=f32)
            scores = jnp.where(valid, scores * HEAD_DIM ** (-0.5), floor_score)
            sink = jnp.sum(jnp.where(sink_lane == par * heads + h, sinks[...], 0.0), axis=1, keepdims=True)
            peak = jnp.maximum(jnp.max(scores, axis=1, keepdims=True), sink)
            raised = jnp.where(valid, jnp.exp(scores - peak), 0.0)
            total = jnp.sum(raised, axis=1, keepdims=True) + jnp.exp(sink - peak)
            weights = (raised / total).astype(bf)
            outs.append(jnp.dot(weights, values, preferred_element_type=f32))
            if h % 2:
                pump(2)
        act_a[b * BLOCK : (b + 1) * BLOCK, :] = jnp.concatenate(outs, axis=1).astype(bf)

    back = jnp.transpose(carry_in[...])
    entry = (back[:state], back[state:])

    def bases(row, c):
        return scaled(row, times(c, reach))

    def grown_entry(c):
        return plus((own[0][0][:, :groups], own[0][1][:, :groups]),
                    times((decay[0][0][:, :groups], decay[0][1][:, :groups]), c))

    cut = (reach[0][:, :groups], reach[1][:, :groups])
    base = [
        scaled(begins[0][:, :groups], times(entry, cut)),
        scaled(begins[1][:, :groups], times(grown_entry(entry), cut)),
    ]
    for g in range(groups):
        u = u_scr[g * GROUP_CH : (g + 1) * GROUP_CH, :]
        down = (tab[g, 2], tab[g, 3])
        chosen = lax.broadcasted_iota(jnp.int32, skip.shape, 1) == first + g
        skips = jnp.sum(jnp.where(chosen, skip[...], 0.0), axis=1, keepdims=True)
        states = []
        for b in range(2):
            at_re = slice(2 * b * state, (2 * b + 1) * state)
            at_im = slice((2 * b + 1) * state, (2 * b + 2) * state)
            p = (prefix[g, at_re] + base[b][0][:, g : g + 1], prefix[g, at_im] + base[b][1][:, g : g + 1])
            states.append(jnp.concatenate(scaled(grows[b, g : g + 1, :], times(down, p)), axis=0))
        high, low = halves(jnp.concatenate(states, axis=1))
        y = jnp.dot(read[g], high, preferred_element_type=f32) + jnp.dot(
            read[g], low, preferred_element_type=f32
        )
        y_scr[g * GROUP_CH : (g + 1) * GROUP_CH, :] = y + skips * u
        if g % 2 == 1:
            pump(2)
    act_s[...] = jnp.transpose(jax.nn.gelu(y_scr[...])).astype(bf)
    pump(len(queue))

    for c in local[13:]:
        c.wait()

    def blocks_of(j):
        return pl.ds(pl.multiple_of(j * cols, 128), cols)

    def multiply(j):
        here = blocks_of(j)
        total = jnp.dot(act_s[...], wo_s[:, here], preferred_element_type=f32) + jnp.dot(
            act_a[...], wo_a[:, here], preferred_element_type=f32
        )
        size = tokens // 2
        for e in range(2):
            for side in range(2):
                block = total[e * tokens + side * size : e * tokens + (side + 1) * size]
                pf[j, e, side] = block
                pb[j, side, e] = block.astype(bf)
        launch(remote(pb.at[j, other], got.at[j], d_s.at[j], d_r.at[j], tp=other))

    def pass_on(j):
        remote(got.at[j], got.at[j], d_s.at[j], d_r.at[j], tp=other).wait_recv()
        fsend[j] = (pf[j, 1 - par, t] + got[j, 1 - par].astype(f32)).astype(bf)
        launch(remote(fsend.at[j], fgot.at[j], e_s.at[j], e_r.at[j], sp=pair))

    def settle(j):
        remote(fgot.at[j], fgot.at[j], e_s.at[j], e_r.at[j], sp=pair).wait_recv()
        total = pf[j, par, t] + got[j, par].astype(f32) + fgot[j].astype(f32)
        res[:, blocks_of(j)] = total.astype(bf)
        launch(pltpu.make_async_copy(res.at[:, blocks_of(j)], out.at[:, blocks_of(j)], o_s.at[j]))

    line = (k,) + order
    for i, j in enumerate(line):
        if i:
            complete(3, j)
            complete(4, j)
        multiply(j)
        if i:
            pass_on(line[i - 1])
    pass_on(line[-1])
    settle(pair)
    settle(k)
    for j in line[2:]:
        settle(j)

    for c in sent:
        if c.is_remote:
            c.wait_send()
        else:
            c.wait()

    @pl.when(late == 0)
    def _():
        hand_kv.wait_send()
        hand_state.wait_send()


def layer(x, gain, ssm, query, key, value, rate, turn, parts, reads, skip, shift, sinks, ows, owa):
    bf, f32 = jnp.bfloat16, jnp.float32
    tokens, half = x.shape
    rows, cols = ows.shape[0], ows.shape[1]
    depth = 4 * ssm.shape[0]
    wide = ssm.shape[1] // 2
    groups, state = rate.shape[0] // 2, rate.shape[1]
    length = 2 * tokens
    dma = pltpu.SemaphoreType.DMA
    vm = pltpu.VMEM
    return pl.pallas_call(
        layer_kernel,
        out_shape=jax.ShapeDtypeStruct((tokens // 2, 4 * cols), bf),
        in_specs=[ANY] * 15,
        out_specs=ANY,
        scratch_shapes=[
            vm((length, 2 * half), bf), vm((length, 2 * half), bf),
            vm((depth, wide), bf), vm((depth, wide), bf), vm((depth, 2 * HEAD_DIM), bf),
            vm((wide, 4 * cols), bf), vm((wide, 4 * cols), bf),
            vm(key.shape, bf), vm(value.shape, bf), vm((2, key.shape[0], 2 * HEAD_DIM), bf),
            vm(gain.shape, f32), vm(rate.shape, f32), vm(turn.shape, f32),
            vm(parts.shape, bf), vm(reads.shape, bf), vm(skip.shape, f32),
            vm((groups, length), f32), vm(sinks.shape, f32),
            vm((groups, 4, state, BLOCK), f32), vm((groups, 2 * state, GROUP_CH), bf),
            vm((groups, GROUP_CH, 2 * state), bf), vm((2, groups, BLOCK), f32), vm((2, groups, BLOCK), f32),
            vm((groups, 4 * state, BLOCK), f32), vm((wide, length), f32), vm((length, wide), bf),
            vm((length + WINDOW, 2 * HEAD_DIM), bf), vm((wide, length), f32),
            vm((length, wide), bf), vm((length, wide), bf),
            vm((groups, 2 * state), f32), vm((groups, 2 * state), f32),
            vm((4, 2, 2, tokens // 2, cols), f32), vm((4, 2, 2, tokens // 2, cols), bf),
            vm((4, 2, tokens // 2, cols), bf), vm((4, tokens // 2, cols), bf), vm((4, tokens // 2, cols), bf),
            vm((tokens // 2, 4 * cols), bf),
            dma((15,)), dma((5, 4)), dma((5, 4)), dma((6,)), dma((6,)),
            dma((5, 4, 2)), dma((5, 4, 2)), dma((5, 4, 2)), dma((5, 4, 2)),
            dma((5, 4)), dma((5, 4)), dma((5, 4)), dma((5, 4)),
            dma((4,)), dma((4,)), dma((4,)), dma((4,)), dma((4,)),
        ],
        compiler_params=pltpu.CompilerParams(collective_id=0, has_side_effects=True),
    )(x, gain, ssm, query, key, value, rate, turn, parts, reads, skip, shift, sinks, ows, owa)


def fast_body(
    inputs, norm_gain, in_ssm, in_query, in_key, in_value, decay_rate, rotation, input_parts,
    output_parts, skip_scale, decay_shift, sink_logit, out_state, out_attend,
):
    return layer(
        inputs, norm_gain[None], in_ssm, in_query, in_key, in_value, decay_rate, rotation,
        jnp.swapaxes(input_parts, 2, 3), output_parts, skip_scale.T, jnp.transpose(decay_shift),
        sink_logit[None], out_state, out_attend,
    )


def body(*args):
    n, n_fs, n_tp = lax.axis_size("sp"), lax.axis_size("fs"), lax.axis_size("tp")
    inputs, in_ssm, in_query, in_key, decay_rate = args[0], args[2], args[3], args[4], args[6]
    key_heads = in_key.shape[1] // HEAD_DIM
    query_heads = in_query.shape[1] // HEAD_DIM
    fits = (
        n_tp == 2
        and n == 4
        and n_fs == 4
        and key_heads == 2
        and query_heads % 4 == 0
        and query_heads * HEAD_DIM == in_ssm.shape[1]
        and in_ssm.shape[1] % 256 == 0
        and in_ssm.shape[1] == args[13].shape[0] == args[14].shape[0]
        and decay_rate.shape[0] % 32 == 0
        and decay_rate.shape[0] <= 2 * BLOCK
        and decay_rate.shape[1] * 2 == BLOCK
        and decay_rate.shape[0] * GROUP_CH == in_ssm.shape[1]
        and inputs.shape[0] == BLOCK == WINDOW
        and inputs.shape[1] % 128 == 0
        and in_ssm.shape[0] % 128 == 0
        and args[13].shape[1] % 128 == 0
    )
    return (fast_body if fits else general_body)(*args)


def solution(mesh):
    return jax.shard_map(
        body,
        mesh=mesh,
        in_specs=(
            P(("fs", "sp"), "tp"),
            P(),
            P("sp", "tp"),
            P("sp", "tp"),
            P("sp", "tp"),
            P("sp", "tp"),
            P("tp", None),
            P("tp", None),
            P(None, "tp", None, None),
            P(None, "tp", None, None),
            P("tp", None),
            P(("fs", "sp"), "tp"),
            P("tp"),
            P("tp", "sp"),
            P("tp", "sp"),
        ),
        out_specs=P(("fs", "sp", "tp"), None),
        check_vma=False,
    )
```

time: 86.8 us -> 65.3 us (0.75)
  Pallas kernels: 80.2 us -> 63 us
  local copies, waits for them, and re-layouts: 5.4 us -> 1.67 us
  other arithmetic: 0.88 us -> 0 us
    pallas_call x3 -> x1, Pallas kernels: 80.2 us -> 63 us  [layer(): pl.pallas_call(layer_kernel, out_shape=jax.ShapeDtypeStruct((tokens // 2,...]
    slice x2 -> x0, local copies, waits for them, and re-layouts: 2.16 us -> none  [fast_body(): array[:, h * HEAD_DIM:(h + 1) * HEAD_DIM]]
    unnamed x3 -> x1, local copies, waits for them, and re-layouts: 2.62 us -> 1.67 us
    another operation x2 -> x0, other arithmetic: 0.88 us -> none  [fast_body(): jnp.stack([jnp.concatenate([array[:, h * HEAD_DIM:(h + 1) * HEAD_DIM] for...]
where the time goes in v1:
time: 65.3 us; the launch traced here: 64.7 us
  Pallas kernels  63 us (96%)
  local copies, waits for them, and re-layouts  1.67 us (3%)
    pallas_call x1, Pallas kernels, layer(): pl.pallas_call(layer_kernel, out_shape=jax.ShapeDtypeStruct((tokens // 2,...  63 us
    unnamed x1, local copies, waits for them, and re-layouts  1.67 us

profile of v1, /device:TPU:0, one launch (start us, length us, event | category | flops | bytes accessed | tf_op | source)
XLA Modules:
  0.0 64.7 jit_solution(990210528103154220)
XLA Ops:
  0.0 63.0 %shard_map.145 = bf16[64,2048]{1,0:T(8,128)(2,1)} custom-call(bf16[128,1024]{1,0:T(8,128)(2,1)} %x_in.1, f32[1,2048]{1,0:T(1,128)} %bitcast.7, bf16[512,512]{1,0:T(8,128)(2,1)} %ssm.1, bf16[512,512]{1,0:T(8,128)(2,1)} %query.1, bf16[512,128]{1,0:T(8,128)(2,1)} %key_in.1, bf16[512,128]{1,0:T(8,128)(2,1)} %value_in.1, f32[32,64]{1,0:T(8,128)} %rate_in.1, ...), custom_call_target="tpu_custom_call" | custom-call | tf_op jit(solution)/shard_map/pallas_call | solution.py:738
  63.0 1.7 %copy.17 = bf16[64,2048]{1,0:T(8,128)(2,1)} copy(bf16[64,2048]{1,0:T(8,128)(2,1)} %shard_map.145) | data formatting | bytes 524288

commit v2 on v1

--- a/solution.py
+++ b/solution.py
@@ -300,47 +300,55 @@
 
 def layer_kernel(x_in, gain_in, ssm, query, key_in, value_in, rate_in, turn_in, parts_in, reads_in,
                  skip_in, shift_in, sinks_in, ows, owa, out,
-                 xf, normed, w_ssm, w_query, w_kv, wo_s, wo_a, key, value, pairs, gain, rate, turn,
+                 xf, xp, normed, w_ssm, w_query, w_key, w_value, wo_s, wo_a, gain, rate, turn,
                  parts, reads, skip, shift, sinks, tab, inm, read, lifts, grows, prefix, u_scr, q_scr,
-                 kv_scr, y_scr, act_s, act_a, carry_out, carry_in, pf, pb, got, fsend, fgot, res,
-                 loc, z_s, z_r, p_s, p_r, ax_s, ax_r, ay_s, ay_r, bx_s, bx_r, by_s, by_r,
-                 d_s, d_r, e_s, e_r, o_s):
+                 kv_scr, y_scr, act_s, act_a, carry_out, carry_in, scale_out, scale_in, total_in,
+                 give_u, give_q, give_kv, got_u, got_q, got_kv, pa, pf, pb, got, fsend, res,
+                 loc, z_s, z_r, p_s, p_r, x_s, x_r, g_s, g_r, d_s, d_r, e_s, e_r, o_s):
     f32, bf = jnp.float32, jnp.bfloat16
     k, f, t = lax.axis_index("sp"), lax.axis_index("fs"), lax.axis_index("tp")
     n, n_fs = 4, 4
     tokens, half = x_in.shape
     rows, cols = ssm.shape[0], ows.shape[1]
-    wide = w_ssm.shape[1]
+    wide = w_ssm.shape[2] // 2
     groups, state = tab.shape[0], tab.shape[2]
-    heads = w_query.shape[1] // HEAD_DIM
+    heads = wide // HEAD_DIM
     par, late = lax.rem(k, 2), lax.div(k, 2)
     pair = k + 1 - 2 * par
-    order = (pair, 2 - late, 3 - 3 * late)
     other = 1 - t
-    fx, fy = f + 1 - 2 * lax.rem(f, 2), lax.rem(f + 2, n_fs)
-    greet([{"sp": j} for j in order] + [{"fs": fx}, {"fs": fy}, {"tp": other}])
-
-    part, height = rows // n_fs, wide // n_fs
-    into = (w_ssm, w_query, w_kv, wo_s, wo_a)
-
-    def region(w, j, q, side=None):
-        size = part if w < 3 else height
-        first = q * size
-        if side is not None:
-            size //= 2
-            first = first + side * size
-        if w < 3:
-            return into[w].at[pl.ds(pl.multiple_of(j * rows + first, 16), size)]
-        return into[w].at[pl.ds(pl.multiple_of(first, 16), size), pl.ds(pl.multiple_of(j * cols, 128), cols)]
-
-    def piece(w, peer):
-        kind = lax.rem(peer, 2)
-        mine = pl.ds(pl.multiple_of(f * part, 16), part)
+    fx, fy, far = f + 1 - 2 * lax.rem(f, 2), lax.rem(f + 2, n_fs), n_fs - 1 - f
+    across_z = lax.rem(k + 2, n)
+
+    part = rows // n_fs
+    into = (w_ssm, w_query, None, wo_s, wo_a)
+    origin = (ssm, query, None, ows, owa)
+    cuts = (4, 2, 2, 2, 2)
+
+    def region(w, c, q, slot):
         if w == 2:
-            return pairs.at[kind, mine]
-        if w < 2:
-            return (ssm, query)[w].at[mine, pl.ds(pl.multiple_of(kind * wide, 128), wide)]
-        return (ows, owa)[w - 3].at[pl.ds(pl.multiple_of(kind * wide + f * height, 16), height)]
+            return (w_key, w_value)[c].at[slot, pl.ds(pl.multiple_of(q * part, 16), part)]
+        size = part // cuts[w]
+        return into[w].at[slot, pl.ds(pl.multiple_of(q * part + c * size, 16), size)]
+
+    def over_z(w, c):
+        if w == 2:
+            source = (key_in, value_in)[c].at[pl.ds(pl.multiple_of(f * part, 16), part)]
+        else:
+            size = part // cuts[w]
+            source = origin[w].at[pl.ds(pl.multiple_of(f * part + c * size, 16), size)]
+        return remote(source, region(w, c, f, late), z_s.at[w, c], z_r.at[w, c], sp=across_z)
+
+    def spread_here(w, c):
+        block = region(w, c, f, 1 - late)
+        remote(block, block, z_s.at[w, c], z_r.at[w, c], sp=across_z).wait_recv()
+        for i, who in enumerate((far, fx, fy)):
+            launch(remote(block, block, x_s.at[w, c, i], x_r.at[w, c, i], fs=who))
+
+    def spread_done(w):
+        for c in range(cuts[w]):
+            for i, who in enumerate((far, fx, fy)):
+                block = region(w, c, who, 1 - late)
+                remote(block, block, x_s.at[w, c, i], x_r.at[w, c, i], fs=who).wait_recv()
 
     sent = []
 
@@ -348,93 +356,30 @@
         c.start()
         sent.append(c)
 
-    def over_z(w, peer):
-        launch(remote(piece(w, peer), region(w, k, f), z_s.at[w, peer], z_r.at[w, k], sp=peer))
-
-    def x_at(e, side):
-        return xf.at[pl.ds(pl.multiple_of(e * tokens, 128), tokens), pl.ds(pl.multiple_of(side * half, 128), half)]
-
     def shift_at(e):
         return shift.at[:, pl.ds(pl.multiple_of(e * tokens, 128), tokens)]
 
     def shift_rows(e):
         return shift_in.at[pl.ds(pl.multiple_of(e * groups, 8), groups)]
 
-    def z_here(w, j):
-        block = region(w, j, f)
-        remote(block, block, z_s.at[w, j], z_r.at[w, j], sp=j).wait_recv()
-        for side in (0, 1):
-            a = region(w, j, f, side)
-            launch(remote(a, a, ax_s.at[w, j, side], ax_r.at[w, j, side], fs=fx))
-            b = region(w, j, f, 1 - side)
-            launch(remote(b, b, ay_s.at[w, j, 1 - side], ay_r.at[w, j, 1 - side], fs=fy))
-
-    def relay(w, j):
-        a = region(w, j, fx, 0)
-        remote(a, a, ax_s.at[w, j, 0], ax_r.at[w, j, 0], fs=fx).wait_recv()
-        launch(remote(a, a, by_s.at[w, j], by_r.at[w, j], fs=fy))
-        b = region(w, j, fy, 1)
-        remote(b, b, ay_s.at[w, j, 1], ay_r.at[w, j, 1], fs=fy).wait_recv()
-        launch(remote(b, b, bx_s.at[w, j], bx_r.at[w, j], fs=fx))
-
-    def complete(w, j):
-        a = region(w, j, fx, 1)
-        remote(a, a, ax_s.at[w, j, 1], ax_r.at[w, j, 1], fs=fx).wait_recv()
-        b = region(w, j, fy, 0)
-        remote(b, b, ay_s.at[w, j, 0], ay_r.at[w, j, 0], fs=fy).wait_recv()
-        far = n_fs - 1 - f
-        a = region(w, j, far, 0)
-        remote(a, a, by_s.at[w, j], by_r.at[w, j], fs=fy).wait_recv()
-        b = region(w, j, far, 1)
-        remote(b, b, bx_s.at[w, j], bx_r.at[w, j], fs=fx).wait_recv()
-
-    def steps_of(ws):
-        steps = []
-        waiting = []
-        for j in order:
-            for w in ws:
-                steps.append(functools.partial(z_here, w, j))
-                if waiting:
-                    steps.append(waiting.pop(0))
-                waiting.append(functools.partial(relay, w, j))
-        return steps + waiting
-
-    queue = steps_of((0,))
+    queue = [(f"s{w}{c}", functools.partial(spread_here, w, c)) for w in (0, 2, 1, 4, 3) for c in range(cuts[w])]
 
     def pump(count):
-        for _ in range(count):
-            if queue:
-                queue.pop(0)()
-
-    for peer in order:
-        over_z(0, peer)
-    launch(remote(x_in, x_at(par, t), p_s.at[0], p_r.at[0], sp=pair))
-    launch(remote(x_in, x_at(par, t), p_s.at[2], p_r.at[2], tp=other))
-    launch(remote(shift_rows(1 - par), shift_at(par), p_s.at[1], p_r.at[1], sp=pair))
-    for peer in order:
-        over_z(1, peer)
-    everything = pl.ds(0, rows)
-    here = pl.ds(pl.multiple_of(k * rows, 16), rows)
-    mine = pl.ds(pl.multiple_of(par * wide, 128), wide)
-    columns = pl.ds(pl.multiple_of(k * cols, 128), cols)
+        for _ in range(min(count, len(queue))):
+            name, step = queue.pop(0)
+            with jax.named_scope(name):
+                step()
+
     local = [
-        (key_in, key), (value_in, value), (rate_in, rate), (turn_in, turn), (parts_in, parts),
-        (reads_in, reads), (skip_in, skip), (gain_in, gain), (sinks_in, sinks),
-        (shift_rows(par), shift_at(par)), (x_in, x_at(par, t)),
-        (ssm.at[everything, mine], w_ssm.at[here]), (query.at[everything, mine], w_query.at[here]),
-        (ows.at[mine], wo_s.at[:, columns]), (owa.at[mine], wo_a.at[:, columns]),
+        (rate_in, rate), (turn_in, turn), (parts_in, parts), (reads_in, reads), (skip_in, skip),
+        (gain_in, gain), (sinks_in, sinks), (shift_rows(par), shift_at(par)),
+        (x_in, xf.at[:, pl.ds(pl.multiple_of(t * half, 128), half)]),
+        (ssm, w_ssm.at[late]), (query, w_query.at[late]), (key_in, w_key.at[late]),
+        (value_in, w_value.at[late]), (ows, wo_s.at[late]), (owa, wo_a.at[late]),
     ]
     local = [pltpu.make_async_copy(a, b, loc.at[i]) for i, (a, b) in enumerate(local)]
     for c in local:
         c.start()
-    local[0].wait()
-    local[1].wait()
-    for e in range(2):
-        span = slice(e * HEAD_DIM, (e + 1) * HEAD_DIM)
-        pairs[e] = jnp.concatenate([key[:, span], value[:, span]], axis=1)
-    w_kv[here, :] = pairs[par]
-    for c in local[2:11]:
-        c.wait()
     first = par * groups
 
     def tables(g, columns_of):
@@ -470,36 +415,95 @@
         return jnp.where(spot, rates, columns_of[0]), jnp.where(spot, turns, columns_of[1])
 
     columns_of = (jnp.zeros((state, BLOCK), f32), jnp.zeros((state, BLOCK), f32))
-    quarter = groups // 4
-    columns_of = lax.fori_loop(0, quarter, tables, columns_of)
-    for i, peer in enumerate(order):
-        over_z(2, peer)
-    for peer in order:
-        over_z(3, peer)
-        over_z(4, peer)
+    early = (n - 1 - k) * (n - 1 - k)
+    peers = [{"sp": pair}, {"sp": across_z}, {"fs": fx}, {"fs": fy}, {"fs": far}, {"tp": other}]
+    barrier = pltpu.get_barrier_semaphore()
+    for peer in peers:
+        pl.semaphore_signal(barrier, inc=1, device_id=peer, device_id_type=MESH)
+
+    def settle_params():
+        for c in local[:8]:
+            c.wait()
+
+    pl.when(k < n - 1)(settle_params)
+    with jax.named_scope("tables"):
+        columns_of = lax.fori_loop(0, early, tables, columns_of)
+    with jax.named_scope("greet"):
+        pl.semaphore_wait(barrier, len(peers))
+    at_end = k * (n - 1 - k) == 0
+    sides = pl.ds(pl.multiple_of(t * half, 128), half)
+    launch(remote(x_in, xf.at[:, sides], p_s.at[0], p_r.at[0], tp=other))
+    launch(remote(x_in.at[:, pl.ds(pl.multiple_of((1 - par) * rows, 128), rows)], xp.at[t],
+                  p_s.at[1], p_r.at[1], sp=pair))
+    launch(remote(shift_rows(1 - par), shift_at(par), p_s.at[2], p_r.at[2], sp=pair))
+    for c in range(cuts[0]):
+        launch(over_z(0, c))
+    pl.when(k == n - 1)(settle_params)
+    with jax.named_scope("tables"):
+        columns_of = lax.fori_loop(early, 10, tables, columns_of)
+
+    local[8].wait()
+    theirs = xf.at[:, pl.ds(pl.multiple_of(other * half, 128), half)]
+    with jax.named_scope("own_x"):
+        remote(theirs, theirs, p_s.at[0], p_r.at[0], tp=other).wait_recv()
+
+    def gain_of(slot):
+        return gain[:, pl.ds(pl.multiple_of((2 * slot + par) * rows, 128), rows)]
+
+    own_rows = pl.ds(pl.multiple_of(par * tokens, 128), tokens)
+    pair_rows = pl.ds(pl.multiple_of((1 - par) * tokens, 128), tokens)
+    with jax.named_scope("norm"):
+        full = xf[...].astype(f32)
+        scale = lax.rsqrt(jnp.mean(full * full, axis=1, keepdims=True) + epsilon)
+        same = lax.broadcasted_iota(jnp.int32, (tokens, tokens), 0) == lax.broadcasted_iota(
+            jnp.int32, (tokens, tokens), 1
+        )
+        line = jnp.sum(jnp.where(same, scale, 0.0), axis=0, keepdims=True)
+        scale_out[...] = jnp.broadcast_to(line, scale_out.shape)
+    launch(remote(scale_out, scale_in, p_s.at[3], p_r.at[3], sp=pair))
+    with jax.named_scope("norm"):
+        for slot in range(2):
+            block = xf[:, pl.ds(pl.multiple_of((2 * slot + par) * rows, 128), rows)].astype(f32)
+            normed[slot, own_rows] = (block * scale * gain_of(slot)).astype(bf)
+    with jax.named_scope("next_x"):
+        remote(xp.at[t], xp.at[t], p_s.at[1], p_r.at[1], sp=pair).wait_recv()
+    launch(remote(xp.at[t], xp.at[t], p_s.at[4], p_r.at[4], tp=other))
     pump(2)
-    columns_of = lax.fori_loop(quarter, 2 * quarter, tables, columns_of)
+    with jax.named_scope("tables"):
+        columns_of = lax.fori_loop(10, 13, tables, columns_of)
+    with jax.named_scope("partner_x"):
+        remote(xp.at[other], xp.at[other], p_s.at[4], p_r.at[4], tp=other).wait_recv()
+        remote(scale_in, scale_in, p_s.at[3], p_r.at[3], sp=pair).wait_recv()
+    with jax.named_scope("norm"):
+        scale = column(scale_in[0:1, :])
+        for slot in range(2):
+            normed[slot, pair_rows] = (xp[slot].astype(f32) * scale * gain_of(slot)).astype(bf)
     pump(2)
-
-    def normalize(e):
-        block = pl.ds(pl.multiple_of(e * tokens, 128), tokens)
-        full = xf[block, :].astype(f32)
-        scale = lax.rsqrt(jnp.mean(full * full, axis=1, keepdims=True) + epsilon)
-        normed[block, :] = (full * scale * gain[...]).astype(bf)
-
-    theirs = x_at(par, other)
-    remote(theirs, theirs, p_s.at[2], p_r.at[2], tp=other).wait_recv()
-    normalize(par)
-    columns_of = lax.fori_loop(2 * quarter, 3 * quarter, tables, columns_of)
-    pump(1)
-    columns_of = lax.fori_loop(3 * quarter, groups, tables, columns_of)
-    pump(len(queue))
-    queue += steps_of((1, 2))
-    next_x = x_at(1 - par, t)
-    remote(next_x, next_x, p_s.at[0], p_r.at[0], sp=pair).wait_recv()
-    launch(remote(next_x, next_x, p_s.at[3], p_r.at[3], tp=other))
-    near = shift_at(1 - par)
-    remote(near, near, p_s.at[1], p_r.at[1], sp=pair).wait_recv()
+    fast = t == 1
+    for c in range(2):
+        launch(over_z(2, c))
+    query_weights = [over_z(1, c) for c in range(2)]
+
+    @pl.when(jnp.logical_not(fast))
+    def _():
+        for c in query_weights:
+            c.start()
+
+    with jax.named_scope("tables"):
+        columns_of = lax.fori_loop(13, groups, tables, columns_of)
+    for c in local[9:]:
+        c.wait()
+    with jax.named_scope("own_u"):
+        total_in[...] = jnp.dot(normed[late], w_ssm[late], preferred_element_type=f32)
+
+    def part_of(w, slot):
+        return jnp.dot(normed[slot], w[slot], preferred_element_type=f32)
+
+    def mine_at(e):
+        return pl.ds(pl.multiple_of(e * wide, 128), wide)
+
+    near_shift = shift_at(1 - par)
+    remote(near_shift, near_shift, p_s.at[2], p_r.at[2], sp=pair).wait_recv()
 
     shape = (BLOCK, BLOCK)
     upto = lax.broadcasted_iota(jnp.int32, shape, 0) <= lax.broadcasted_iota(jnp.int32, shape, 1)
@@ -546,61 +550,109 @@
     reach, end = spiral(centre + 1.0), spiral(BLOCK - 1.0 - centre)
     whole = times(reach, end)
 
-    theirs = x_at(1 - par, other)
-    remote(theirs, theirs, p_s.at[3], p_r.at[3], tp=other).wait_recv()
-    normalize(1 - par)
-    local[11].wait()
-    for j in order:
-        complete(0, j)
-    u = jnp.dot(normed[...], w_ssm[...], preferred_element_type=f32)
-    u_scr[...] = jnp.transpose(u.astype(bf).astype(f32))
+    pump(2)
+
+    @pl.when(fast)
+    def _():
+        for c in query_weights:
+            c.start()
+
+    sent.extend(query_weights)
+    with jax.named_scope("ssm_wait"):
+        spread_done(0)
+    with jax.named_scope("project_u"):
+        total_in[...] += part_of(w_ssm, 1 - late)
+        give_u[...] = total_in[:, mine_at(1 - par)].astype(bf)
+    launch(remote(give_u, got_u, g_s.at[0], g_r.at[0], sp=pair))
+    pump(2)
+    for c in range(2):
+        launch(over_z(4, c))
+    def query_parts():
+        with jax.named_scope("query_wait"):
+            spread_done(1)
+        with jax.named_scope("project_q"):
+            total_in[...] = part_of(w_query, 0) + part_of(w_query, 1)
+            give_q[...] = total_in[:, mine_at(1 - par)].astype(bf)
+        launch(remote(give_q, got_q, g_s.at[1], g_r.at[1], sp=pair))
+
+    def key_parts():
+        with jax.named_scope("key_wait"):
+            spread_done(2)
+        with jax.named_scope("project_kv"):
+            keys = part_of(w_key, 0) + part_of(w_key, 1)
+            values = part_of(w_value, 0) + part_of(w_value, 1)
+            both = [
+                jnp.concatenate([a[:, e * HEAD_DIM : (e + 1) * HEAD_DIM] for a in (keys, values)], axis=1)
+                for e in range(2)
+            ]
+            give_kv[...] = jnp.where(par == 0, both[1], both[0]).astype(bf)
+        launch(remote(give_kv, got_kv, g_s.at[2], g_r.at[2], sp=pair))
+
+        return jnp.where(par == 0, both[0], both[1])
+
+    own_kv = key_parts()
+    with jax.named_scope("got_u"):
+        remote(got_u, got_u, g_s.at[0], g_r.at[0], sp=pair).wait_recv()
+    with jax.named_scope("turn_u"):
+        u = total_in[:, mine_at(par)] + got_u[...].astype(f32)
+        u_scr[...] = jnp.transpose(u.astype(bf).astype(f32))
+
+    tail = kv_scr.at[pl.ds(2 * WINDOW, WINDOW)]
+    head = kv_scr.at[pl.ds(0, WINDOW)]
+    hand_kv = remote(tail, head, p_s.at[5], p_r.at[5], sp=across_z)
+    hand_state = remote(carry_out, carry_in, p_s.at[6], p_r.at[6], sp=across_z)
+
+    def settle_kv():
+        with jax.named_scope("kv_wait"):
+            remote(got_kv, got_kv, g_s.at[2], g_r.at[2], sp=pair).wait_recv()
+        kv_scr[WINDOW:, :] = (own_kv + got_kv[...].astype(f32)).astype(bf)
+
+        @pl.when(late == 0)
+        def _():
+            hand_kv.start()
+            kv_scr[:WINDOW, :] = jnp.zeros((WINDOW, kv_scr.shape[1]), bf)
 
     lane = lax.broadcasted_iota(jnp.int32, (state, BLOCK), 1)
     ends = [jnp.zeros((state, BLOCK), f32)] * 4
     for g in range(groups):
-        u = u_scr[g * GROUP_CH : (g + 1) * GROUP_CH, :]
-        drive = jnp.dot(inm[g], u.astype(bf), preferred_element_type=f32)
-        up_re, up_im = tab[g, 0], tab[g, 1]
-        lifted = []
-        for b in range(2):
-            span = slice(b * BLOCK, (b + 1) * BLOCK)
-            row = lifts[b, g : g + 1, :]
-            d_re, d_im = drive[:state, span] * row, drive[state:, span] * row
-            lifted += [d_re * up_re - d_im * up_im, d_re * up_im + d_im * up_re]
-        sums = split_dot(jnp.concatenate(lifted, axis=0), tri)
-        prefix[g] = sums
-        ends = [
-            jnp.where(lane == g, sums[i * state : (i + 1) * state, BLOCK - 1 :], ends[i])
-            for i in range(4)
-        ]
-        if g % 2 == 1:
-            pump(2)
-    pump(len(queue))
-    queue += steps_of((3, 4))
-    own = [scaled(lasts[b], times(end, (ends[2 * b], ends[2 * b + 1]))) for b in range(2)]
-    decay = [scaled(lasts[b] * begins[b], whole) for b in range(2)]
-    final = plus(own[1], times(decay[1], own[0]))
-    carry_out[...] = jnp.transpose(jnp.concatenate(final, axis=0))[:groups]
-
-    local[12].wait()
-    for w in (1, 2):
-        for j in order:
-            complete(w, j)
-    kv_scr[WINDOW:, :] = jnp.dot(normed[...], w_kv[...], preferred_element_type=f32).astype(bf)
-    q_scr[...] = jnp.dot(normed[...], w_query[...], preferred_element_type=f32).astype(bf)
-    ahead, behind = lax.rem(k + 2, n), lax.rem(k + 2, n)
-    tail = kv_scr.at[pl.ds(2 * WINDOW, WINDOW)]
-    head = kv_scr.at[pl.ds(0, WINDOW)]
-    hand_kv = remote(tail, head, p_s.at[4], p_r.at[4], sp=ahead)
-    hand_state = remote(carry_out, carry_in, p_s.at[5], p_r.at[5], sp=ahead)
+        with jax.named_scope("first"):
+            u = u_scr[g * GROUP_CH : (g + 1) * GROUP_CH, :]
+            drive = jnp.dot(inm[g], u.astype(bf), preferred_element_type=f32)
+            up_re, up_im = tab[g, 0], tab[g, 1]
+            lifted = []
+            for b in range(2):
+                span = slice(b * BLOCK, (b + 1) * BLOCK)
+                row = lifts[b, g : g + 1, :]
+                d_re, d_im = drive[:state, span] * row, drive[state:, span] * row
+                lifted += [d_re * up_re - d_im * up_im, d_re * up_im + d_im * up_re]
+            sums = split_dot(jnp.concatenate(lifted, axis=0), tri)
+            prefix[g] = sums
+            ends = [
+                jnp.where(lane == g, sums[i * state : (i + 1) * state, BLOCK - 1 :], ends[i])
+                for i in range(4)
+            ]
+        if g == 5:
+            settle_kv()
+        if g == 9:
+            query_parts()
+        if g in (11, 14):
+            pump(1)
+    with jax.named_scope("carry"):
+        own = [scaled(lasts[b], times(end, (ends[2 * b], ends[2 * b + 1]))) for b in range(2)]
+        decay = [scaled(lasts[b] * begins[b], whole) for b in range(2)]
+        final = plus(own[1], times(decay[1], own[0]))
+        carry_out[...] = jnp.transpose(jnp.concatenate(final, axis=0))[:groups]
 
     @pl.when(late == 0)
     def _():
-        hand_kv.start()
         hand_state.start()
-        kv_scr[:WINDOW, :] = jnp.zeros((WINDOW, kv_scr.shape[1]), bf)
         carry_in[...] = jnp.zeros(carry_in.shape, f32)
 
+    for c in range(2):
+        launch(over_z(3, c))
+    with jax.named_scope("q_wait"):
+        remote(got_q, got_q, g_s.at[1], g_r.at[1], sp=pair).wait_recv()
+    q_scr[...] = (total_in[:, mine_at(par)] + got_q[...].astype(f32)).astype(bf)
     gap_shape = (WINDOW, 2 * WINDOW)
     at = lax.broadcasted_iota(jnp.int32, gap_shape, 1)
     gap = lax.broadcasted_iota(jnp.int32, gap_shape, 0) + WINDOW - at
@@ -612,27 +664,31 @@
 
             @pl.when(late == 1)
             def _():
-                hand_kv.wait_recv()
-                hand_state.wait_recv()
+                with jax.named_scope("hand_wait"):
+                    hand_kv.wait_recv()
+                    hand_state.wait_recv()
 
         keys = kv_scr[b * WINDOW : (b + 2) * WINDOW, :HEAD_DIM]
         values = kv_scr[b * WINDOW : (b + 2) * WINDOW, HEAD_DIM:]
         valid = inside if b else inside_first
         outs = []
         for h in range(heads):
-            q = q_scr[b * WINDOW : (b + 1) * WINDOW, h * HEAD_DIM : (h + 1) * HEAD_DIM]
-            scores = lax.dot_general(q, keys, (((1,), (1,)), ((), ())), preferred_element_type=f32)
-            scores = jnp.where(valid, scores * HEAD_DIM ** (-0.5), floor_score)
-            sink = jnp.sum(jnp.where(sink_lane == par * heads + h, sinks[...], 0.0), axis=1, keepdims=True)
-            peak = jnp.maximum(jnp.max(scores, axis=1, keepdims=True), sink)
-            raised = jnp.where(valid, jnp.exp(scores - peak), 0.0)
-            total = jnp.sum(raised, axis=1, keepdims=True) + jnp.exp(sink - peak)
-            weights = (raised / total).astype(bf)
-            outs.append(jnp.dot(weights, values, preferred_element_type=f32))
-            if h % 2:
-                pump(2)
-        act_a[b * BLOCK : (b + 1) * BLOCK, :] = jnp.concatenate(outs, axis=1).astype(bf)
-
+            with jax.named_scope("head"):
+                q = q_scr[b * WINDOW : (b + 1) * WINDOW, h * HEAD_DIM : (h + 1) * HEAD_DIM]
+                scores = lax.dot_general(q, keys, (((1,), (1,)), ((), ())), preferred_element_type=f32)
+                scores = jnp.where(valid, scores * HEAD_DIM ** (-0.5), floor_score)
+                sink = jnp.sum(jnp.where(sink_lane == par * heads + h, sinks[...], 0.0), axis=1, keepdims=True)
+                peak = jnp.maximum(jnp.max(scores, axis=1, keepdims=True), sink)
+                raised = jnp.where(valid, jnp.exp(scores - peak), 0.0)
+                total = jnp.sum(raised, axis=1, keepdims=True) + jnp.exp(sink - peak)
+                weights = (raised / total).astype(bf)
+                outs.append(jnp.dot(weights, values, preferred_element_type=f32))
+            if h == 2 and b == 0:
+                pump(1)
+        act_a[par, b * BLOCK : (b + 1) * BLOCK, :] = jnp.concatenate(outs, axis=1).astype(bf)
+
+    mix_a = remote(act_a.at[par], act_a.at[par], e_s.at[4], e_r.at[4], sp=pair)
+    launch(mix_a)
     back = jnp.transpose(carry_in[...])
     entry = (back[:state], back[state:])
 
@@ -649,75 +705,103 @@
         scaled(begins[1][:, :groups], times(grown_entry(entry), cut)),
     ]
     for g in range(groups):
-        u = u_scr[g * GROUP_CH : (g + 1) * GROUP_CH, :]
-        down = (tab[g, 2], tab[g, 3])
-        chosen = lax.broadcasted_iota(jnp.int32, skip.shape, 1) == first + g
-        skips = jnp.sum(jnp.where(chosen, skip[...], 0.0), axis=1, keepdims=True)
-        states = []
-        for b in range(2):
-            at_re = slice(2 * b * state, (2 * b + 1) * state)
-            at_im = slice((2 * b + 1) * state, (2 * b + 2) * state)
-            p = (prefix[g, at_re] + base[b][0][:, g : g + 1], prefix[g, at_im] + base[b][1][:, g : g + 1])
-            states.append(jnp.concatenate(scaled(grows[b, g : g + 1, :], times(down, p)), axis=0))
-        high, low = halves(jnp.concatenate(states, axis=1))
-        y = jnp.dot(read[g], high, preferred_element_type=f32) + jnp.dot(
-            read[g], low, preferred_element_type=f32
-        )
-        y_scr[g * GROUP_CH : (g + 1) * GROUP_CH, :] = y + skips * u
-        if g % 2 == 1:
-            pump(2)
-    act_s[...] = jnp.transpose(jax.nn.gelu(y_scr[...])).astype(bf)
+        with jax.named_scope("second"):
+            u = u_scr[g * GROUP_CH : (g + 1) * GROUP_CH, :]
+            down = (tab[g, 2], tab[g, 3])
+            chosen = lax.broadcasted_iota(jnp.int32, skip.shape, 1) == first + g
+            skips = jnp.sum(jnp.where(chosen, skip[...], 0.0), axis=1, keepdims=True)
+            states = []
+            for b in range(2):
+                at_re = slice(2 * b * state, (2 * b + 1) * state)
+                at_im = slice((2 * b + 1) * state, (2 * b + 2) * state)
+                p = (prefix[g, at_re] + base[b][0][:, g : g + 1], prefix[g, at_im] + base[b][1][:, g : g + 1])
+                states.append(jnp.concatenate(scaled(grows[b, g : g + 1, :], times(down, p)), axis=0))
+            high, low = halves(jnp.concatenate(states, axis=1))
+            y = jnp.dot(read[g], high, preferred_element_type=f32) + jnp.dot(
+                read[g], low, preferred_element_type=f32
+            )
+            y_scr[g * GROUP_CH : (g + 1) * GROUP_CH, :] = y + skips * u
+        if g == 7:
+            pump(1)
+        if (g + 1) % (groups // 2) == 0:
+            side = (g + 1) // (groups // 2) - 1
+            lanes = slice(side * BLOCK, (side + 1) * BLOCK)
+            with jax.named_scope("gelu"):
+                act_s[par, :, lanes] = jnp.transpose(jax.nn.gelu(y_scr[lanes, :])).astype(bf)
+            half_s = act_s.at[par, :, pl.ds(side * BLOCK, BLOCK)]
+            launch(remote(half_s, half_s, e_s.at[5 + side], e_r.at[5 + side], sp=pair))
+
+    size, chunk = tokens // 2, cols // 2
+    theirs = act_a.at[1 - par]
+    with jax.named_scope("mix_a"):
+        remote(theirs, theirs, e_s.at[4], e_r.at[4], sp=pair).wait_recv()
     pump(len(queue))
 
-    for c in local[13:]:
-        c.wait()
-
-    def blocks_of(j):
-        return pl.ds(pl.multiple_of(j * cols, 128), cols)
-
-    def multiply(j):
-        here = blocks_of(j)
-        total = jnp.dot(act_s[...], wo_s[:, here], preferred_element_type=f32) + jnp.dot(
-            act_a[...], wo_a[:, here], preferred_element_type=f32
-        )
-        size = tokens // 2
+    def attend_part(slot):
+        for side in range(2):
+            lanes = slice(side * chunk, (side + 1) * chunk)
+            rows_a = [jnp.dot(act_a[e], wo_a[slot, e * wide : (e + 1) * wide, lanes], preferred_element_type=f32)
+                      for e in range(2)]
+            pa[slot, :, lanes] = rows_a[0] + rows_a[1]
+
+    with jax.named_scope("attend"):
+        attend_part(late)
+    with jax.named_scope("out_wait"):
+        spread_done(4)
+    with jax.named_scope("attend"):
+        attend_part(1 - late)
+    with jax.named_scope("mix_s"):
+        for side in range(2):
+            theirs = act_s.at[1 - par, :, pl.ds(side * BLOCK, BLOCK)]
+            remote(theirs, theirs, e_s.at[5 + side], e_r.at[5 + side], sp=pair).wait_recv()
+
+    def target(who, i):
+        first_column = lax.rem(who + 2 * (i // 2), n) * cols + (i % 2) * chunk
+        return out.at[:, pl.ds(pl.multiple_of(first_column, 128), chunk)]
+
+    def multiply(i):
+        slot, lanes = late if i < 2 else 1 - late, slice(i % 2 * chunk, (i % 2 + 1) * chunk)
+        total = pa[slot, :, lanes]
+        for e in range(2):
+            total = total + jnp.dot(
+                act_s[e], wo_s[slot, e * wide : (e + 1) * wide, lanes], preferred_element_type=f32
+            )
         for e in range(2):
             for side in range(2):
                 block = total[e * tokens + side * size : e * tokens + (side + 1) * size]
-                pf[j, e, side] = block
-                pb[j, side, e] = block.astype(bf)
-        launch(remote(pb.at[j, other], got.at[j], d_s.at[j], d_r.at[j], tp=other))
-
-    def pass_on(j):
-        remote(got.at[j], got.at[j], d_s.at[j], d_r.at[j], tp=other).wait_recv()
-        fsend[j] = (pf[j, 1 - par, t] + got[j, 1 - par].astype(f32)).astype(bf)
-        launch(remote(fsend.at[j], fgot.at[j], e_s.at[j], e_r.at[j], sp=pair))
-
-    def settle(j):
-        remote(fgot.at[j], fgot.at[j], e_s.at[j], e_r.at[j], sp=pair).wait_recv()
-        total = pf[j, par, t] + got[j, par].astype(f32) + fgot[j].astype(f32)
-        res[:, blocks_of(j)] = total.astype(bf)
-        launch(pltpu.make_async_copy(res.at[:, blocks_of(j)], out.at[:, blocks_of(j)], o_s.at[j]))
-
-    line = (k,) + order
-    for i, j in enumerate(line):
+                pf[i, e, side] = block
+                pb[i, side, e] = block.astype(bf)
+        launch(remote(pb.at[i, other], got.at[i], d_s.at[i], d_r.at[i], tp=other))
+
+    def pass_on(i):
+        remote(got.at[i], got.at[i], d_s.at[i], d_r.at[i], tp=other).wait_recv()
+        fsend[i] = (pf[i, 1 - par, t] + got[i, 1 - par].astype(f32)).astype(bf)
+        launch(remote(fsend.at[i], target(k, i), e_s.at[i], e_r.at[i], sp=pair))
+        res[i] = (pf[i, par, t] + got[i, par].astype(f32)).astype(bf)
+        launch(pltpu.make_async_copy(res.at[i], target(k, i), o_s.at[i]))
+
+    for i in range(4):
+        if i == 2:
+            with jax.named_scope("out_wait"):
+                spread_done(3)
+        with jax.named_scope("multiply"):
+            multiply(i)
         if i:
-            complete(3, j)
-            complete(4, j)
-        multiply(j)
-        if i:
-            pass_on(line[i - 1])
-    pass_on(line[-1])
-    settle(pair)
-    settle(k)
-    for j in line[2:]:
-        settle(j)
-
-    for c in sent:
-        if c.is_remote:
-            c.wait_send()
-        else:
-            c.wait()
+            with jax.named_scope("pass"):
+                pass_on(i - 1)
+    with jax.named_scope("pass"):
+        pass_on(3)
+    with jax.named_scope("settle"):
+        for i in range(4):
+            theirs = target(pair, i)
+            remote(theirs, theirs, e_s.at[i], e_r.at[i], sp=pair).wait_recv()
+
+    with jax.named_scope("drain"):
+        for c in sent:
+            if c.is_remote:
+                c.wait_send()
+            else:
+                c.wait()
 
     @pl.when(late == 0)
     def _():
@@ -729,7 +813,6 @@
     bf, f32 = jnp.bfloat16, jnp.float32
     tokens, half = x.shape
     rows, cols = ows.shape[0], ows.shape[1]
-    depth = 4 * ssm.shape[0]
     wide = ssm.shape[1] // 2
     groups, state = rate.shape[0] // 2, rate.shape[1]
     length = 2 * tokens
@@ -741,10 +824,9 @@
         in_specs=[ANY] * 15,
         out_specs=ANY,
         scratch_shapes=[
-            vm((length, 2 * half), bf), vm((length, 2 * half), bf),
-            vm((depth, wide), bf), vm((depth, wide), bf), vm((depth, 2 * HEAD_DIM), bf),
-            vm((wide, 4 * cols), bf), vm((wide, 4 * cols), bf),
-            vm(key.shape, bf), vm(value.shape, bf), vm((2, key.shape[0], 2 * HEAD_DIM), bf),
+            vm((tokens, 2 * half), bf), vm((2, tokens, rows), bf), vm((2, length, rows), bf),
+            vm((2, rows, 2 * wide), bf), vm((2, rows, 2 * wide), bf), vm((2,) + key.shape, bf),
+            vm((2,) + value.shape, bf), vm((2, rows, cols), bf), vm((2, rows, cols), bf),
             vm(gain.shape, f32), vm(rate.shape, f32), vm(turn.shape, f32),
             vm(parts.shape, bf), vm(reads.shape, bf), vm(skip.shape, f32),
             vm((groups, length), f32), vm(sinks.shape, f32),
@@ -752,15 +834,17 @@
             vm((groups, GROUP_CH, 2 * state), bf), vm((2, groups, BLOCK), f32), vm((2, groups, BLOCK), f32),
             vm((groups, 4 * state, BLOCK), f32), vm((wide, length), f32), vm((length, wide), bf),
             vm((length + WINDOW, 2 * HEAD_DIM), bf), vm((wide, length), f32),
-            vm((length, wide), bf), vm((length, wide), bf),
+            vm((2, length, wide), bf), vm((2, length, wide), bf),
             vm((groups, 2 * state), f32), vm((groups, 2 * state), f32),
-            vm((4, 2, 2, tokens // 2, cols), f32), vm((4, 2, 2, tokens // 2, cols), bf),
-            vm((4, 2, tokens // 2, cols), bf), vm((4, tokens // 2, cols), bf), vm((4, tokens // 2, cols), bf),
-            vm((tokens // 2, 4 * cols), bf),
-            dma((15,)), dma((5, 4)), dma((5, 4)), dma((6,)), dma((6,)),
-            dma((5, 4, 2)), dma((5, 4, 2)), dma((5, 4, 2)), dma((5, 4, 2)),
-            dma((5, 4)), dma((5, 4)), dma((5, 4)), dma((5, 4)),
-            dma((4,)), dma((4,)), dma((4,)), dma((4,)), dma((4,)),
+            vm((8, tokens), f32), vm((8, tokens), f32), vm((length, 2 * wide), f32),
+            vm((length, wide), bf), vm((length, wide), bf), vm((length, 2 * HEAD_DIM), bf),
+            vm((length, wide), bf), vm((length, wide), bf), vm((length, 2 * HEAD_DIM), bf),
+            vm((2, length, cols), f32),
+            vm((4, 2, 2, tokens // 2, cols // 2), f32), vm((4, 2, 2, tokens // 2, cols // 2), bf),
+            vm((4, 2, tokens // 2, cols // 2), bf), vm((4, tokens // 2, cols // 2), bf),
+            vm((4, tokens // 2, cols // 2), bf),
+            dma((15,)), dma((5, 4)), dma((5, 4)), dma((7,)), dma((7,)), dma((5, 4, 3)), dma((5, 4, 3)),
+            dma((3,)), dma((3,)), dma((4,)), dma((4,)), dma((7,)), dma((7,)), dma((4,)),
         ],
         compiler_params=pltpu.CompilerParams(collective_id=0, has_side_effects=True),
     )(x, gain, ssm, query, key, value, rate, turn, parts, reads, skip, shift, sinks, ows, owa)
@@ -798,6 +882,8 @@
         and inputs.shape[0] == BLOCK == WINDOW
         and inputs.shape[1] % 128 == 0
         and in_ssm.shape[0] % 128 == 0
+        and in_ssm.shape[0] == args[13].shape[0]
+        and inputs.shape[1] == 2 * in_ssm.shape[0]
         and args[13].shape[1] % 128 == 0
     )
     return (fast_body if fits else general_body)(*args)

time: 65.3 us -> 55.8 us (0.85)
  Pallas kernels: 63 us -> 53.9 us
    pallas_call x1, Pallas kernels: 63 us -> 53.9 us  [layer(): pl.pallas_call(layer_kernel, out_shape=jax.ShapeDtypeStruct((tokens // 2,...]
where the time goes in v2:
time: 55.8 us; the launch traced here: 55.6 us
  Pallas kernels  53.9 us (97%)
  local copies, waits for them, and re-layouts  1.67 us (3%)
    pallas_call x1, Pallas kernels, layer(): pl.pallas_call(layer_kernel, out_shape=jax.ShapeDtypeStruct((tokens // 2,...  53.9 us
    unnamed x1, local copies, waits for them, and re-layouts  1.67 us

profile of v2, /device:TPU:0, one launch (start us, length us, event | category | flops | bytes accessed | tf_op | source)
XLA Modules:
  0.0 55.6 jit_solution(14630372980158989852)
XLA Ops:
  0.0 53.9 %shard_map.145 = bf16[64,2048]{1,0:T(8,128)(2,1)} custom-call(bf16[128,1024]{1,0:T(8,128)(2,1)} %x_in.1, f32[1,2048]{1,0:T(1,128)} %bitcast.7, bf16[512,512]{1,0:T(8,128)(2,1)} %ssm.1, bf16[512,512]{1,0:T(8,128)(2,1)} %query.1, bf16[512,128]{1,0:T(8,128)(2,1)} %key_in.1, bf16[512,128]{1,0:T(8,128)(2,1)} %value_in.1, f32[32,64]{1,0:T(8,128)} %rate_in.1, ...), custom_call_target="tpu_custom_call" | custom-call | tf_op jit(solution)/shard_map/pallas_call | solution.py:821
  53.9 1.7 %copy.17 = bf16[64,2048]{1,0:T(8,128)(2,1)} copy(bf16[64,2048]{1,0:T(8,128)(2,1)} %shard_map.145) | data formatting | bytes 524288

commit v3 on v2

--- a/solution.py
+++ b/solution.py
@@ -298,11 +298,25 @@
     return jnp.sum(jnp.where(same, row, 0.0), axis=1, keepdims=True)
 
 
+def turned(angle):
+    quarter = jnp.floor(angle * (2.0 / 3.141592653589793) + 0.5)
+    r = ((angle - quarter * 1.5703125) - quarter * 4.837512969970703e-4) - quarter * 7.549789948768648e-8
+    sq = r * r
+    sin = r + r * sq * (-1.6666654611e-1 + sq * (8.3321608736e-3 + sq * -1.9515295891e-4))
+    cos = 1.0 - 0.5 * sq + sq * sq * (4.166664568298827e-2 + sq * (-1.388731625493765e-3 + sq * 2.443315711809948e-5))
+    which = quarter.astype(jnp.int32)
+    swap = (which & 1) == 1
+    flip_cos = ((which + 1) & 2) == 2
+    flip_sin = (which & 2) == 2
+    a, b = jnp.where(swap, sin, cos), jnp.where(swap, cos, sin)
+    return jnp.where(flip_cos, -a, a), jnp.where(flip_sin, -b, b)
+
+
 def layer_kernel(x_in, gain_in, ssm, query, key_in, value_in, rate_in, turn_in, parts_in, reads_in,
                  skip_in, shift_in, sinks_in, ows, owa, out,
                  xf, xp, normed, w_ssm, w_query, w_key, w_value, wo_s, wo_a, gain, rate, turn,
                  parts, reads, skip, shift, sinks, tab, inm, read, lifts, grows, prefix, u_scr, q_scr,
-                 kv_scr, y_scr, act_s, act_a, carry_out, carry_in, scale_out, scale_in, total_in,
+                 kv_scr, y_scr, act_s, act_a, carry_out, carry_in, scale_out, scale_in, total_in, total_q,
                  give_u, give_q, give_kv, got_u, got_q, got_kv, pa, pf, pb, got, fsend, res,
                  loc, z_s, z_r, p_s, p_r, x_s, x_r, g_s, g_r, d_s, d_r, e_s, e_r, o_s):
     f32, bf = jnp.float32, jnp.bfloat16
@@ -322,16 +336,23 @@
     part = rows // n_fs
     into = (w_ssm, w_query, None, wo_s, wo_a)
     origin = (ssm, query, None, ows, owa)
-    cuts = (4, 2, 2, 2, 2)
+    cuts = (4, 4, 2, 2, 2)
+
+    def stripe(c):
+        return pl.ds(c % 2 * wide + c // 2 * (wide // 2), wide // 2)
 
     def region(w, c, q, slot):
+        if w < 2:
+            return into[w].at[slot, pl.ds(pl.multiple_of(q * part, 16), part), stripe(c)]
         if w == 2:
             return (w_key, w_value)[c].at[slot, pl.ds(pl.multiple_of(q * part, 16), part)]
         size = part // cuts[w]
         return into[w].at[slot, pl.ds(pl.multiple_of(q * part + c * size, 16), size)]
 
     def over_z(w, c):
-        if w == 2:
+        if w < 2:
+            source = origin[w].at[pl.ds(pl.multiple_of(f * part, 16), part), stripe(c)]
+        elif w == 2:
             source = (key_in, value_in)[c].at[pl.ds(pl.multiple_of(f * part, 16), part)]
         else:
             size = part // cuts[w]
@@ -344,8 +365,8 @@
         for i, who in enumerate((far, fx, fy)):
             launch(remote(block, block, x_s.at[w, c, i], x_r.at[w, c, i], fs=who))
 
-    def spread_done(w):
-        for c in range(cuts[w]):
+    def spread_done(w, pieces=None):
+        for c in pieces or range(cuts[w]):
             for i, who in enumerate((far, fx, fy)):
                 block = region(w, c, who, 1 - late)
                 remote(block, block, x_s.at[w, c, i], x_r.at[w, c, i], fs=who).wait_recv()
@@ -362,7 +383,7 @@
     def shift_rows(e):
         return shift_in.at[pl.ds(pl.multiple_of(e * groups, 8), groups)]
 
-    queue = [(f"s{w}{c}", functools.partial(spread_here, w, c)) for w in (0, 2, 1, 4, 3) for c in range(cuts[w])]
+    queue = [(f"s{w}{c}", functools.partial(spread_here, w, c)) for w in (0, 2, 1, 3, 4) for c in range(cuts[w])]
 
     def pump(count):
         for _ in range(min(count, len(queue))):
@@ -387,7 +408,7 @@
         rates, turns = column(line), column(spin)
         away = lax.broadcasted_iota(jnp.int32, (state, BLOCK), 1).astype(f32) - float(BLOCK // 2)
         angle = turns * away
-        cos, sin = jnp.cos(angle), jnp.sin(angle)
+        cos, sin = turned(angle)
         fade = jnp.exp(-rates * away)
         rise = jnp.exp(rates * away)
         tab[g, 0] = rise * cos
@@ -433,11 +454,27 @@
     at_end = k * (n - 1 - k) == 0
     sides = pl.ds(pl.multiple_of(t * half, 128), half)
     launch(remote(x_in, xf.at[:, sides], p_s.at[0], p_r.at[0], tp=other))
-    launch(remote(x_in.at[:, pl.ds(pl.multiple_of((1 - par) * rows, 128), rows)], xp.at[t],
-                  p_s.at[1], p_r.at[1], sp=pair))
+    slow, fast = t == 0, t == 1
+
+    def launch_if(choice, copies):
+        @pl.when(choice)
+        def _():
+            for c in copies:
+                c.start()
+
+    state_weights = [over_z(0, c) for c in range(cuts[0])]
+    early_keys = [over_z(2, c) for c in range(2)]
+    query_weights = [over_z(1, c) for c in range(cuts[1])]
+    out_weights = [over_z(3, c) for c in range(2)]
+    attend_weights = [over_z(4, c) for c in range(2)]
+    give_x = remote(x_in.at[:, pl.ds(pl.multiple_of((1 - par) * rows, 128), rows)], xp.at[t],
+                    p_s.at[1], p_r.at[1], sp=pair)
+    state_weights[0].start()
+    launch_if(slow, state_weights[1:])
     launch(remote(shift_rows(1 - par), shift_at(par), p_s.at[2], p_r.at[2], sp=pair))
-    for c in range(cuts[0]):
-        launch(over_z(0, c))
+    launch_if(slow | jnp.logical_not(at_end), [give_x])
+    launch_if(slow, early_keys)
+    sent.extend(state_weights + early_keys + query_weights + out_weights + attend_weights + [give_x])
     pl.when(k == n - 1)(settle_params)
     with jax.named_scope("tables"):
         columns_of = lax.fori_loop(early, 10, tables, columns_of)
@@ -460,17 +497,23 @@
         )
         line = jnp.sum(jnp.where(same, scale, 0.0), axis=0, keepdims=True)
         scale_out[...] = jnp.broadcast_to(line, scale_out.shape)
+    launch_if(fast, state_weights[1:])
+    launch_if(fast & at_end, [give_x])
     launch(remote(scale_out, scale_in, p_s.at[3], p_r.at[3], sp=pair))
     with jax.named_scope("norm"):
         for slot in range(2):
             block = xf[:, pl.ds(pl.multiple_of((2 * slot + par) * rows, 128), rows)].astype(f32)
             normed[slot, own_rows] = (block * scale * gain_of(slot)).astype(bf)
+    with jax.named_scope("tables"):
+        columns_of = lax.fori_loop(10, groups, tables, columns_of)
+    pump(2)
+    launch_if(fast, early_keys)
+    launch_if(slow, query_weights)
+    pump(2)
+    launch_if(fast, query_weights)
     with jax.named_scope("next_x"):
         remote(xp.at[t], xp.at[t], p_s.at[1], p_r.at[1], sp=pair).wait_recv()
     launch(remote(xp.at[t], xp.at[t], p_s.at[4], p_r.at[4], tp=other))
-    pump(2)
-    with jax.named_scope("tables"):
-        columns_of = lax.fori_loop(10, 13, tables, columns_of)
     with jax.named_scope("partner_x"):
         remote(xp.at[other], xp.at[other], p_s.at[4], p_r.at[4], tp=other).wait_recv()
         remote(scale_in, scale_in, p_s.at[3], p_r.at[3], sp=pair).wait_recv()
@@ -478,19 +521,6 @@
         scale = column(scale_in[0:1, :])
         for slot in range(2):
             normed[slot, pair_rows] = (xp[slot].astype(f32) * scale * gain_of(slot)).astype(bf)
-    pump(2)
-    fast = t == 1
-    for c in range(2):
-        launch(over_z(2, c))
-    query_weights = [over_z(1, c) for c in range(2)]
-
-    @pl.when(jnp.logical_not(fast))
-    def _():
-        for c in query_weights:
-            c.start()
-
-    with jax.named_scope("tables"):
-        columns_of = lax.fori_loop(13, groups, tables, columns_of)
     for c in local[9:]:
         c.wait()
     with jax.named_scope("own_u"):
@@ -508,6 +538,9 @@
     shape = (BLOCK, BLOCK)
     upto = lax.broadcasted_iota(jnp.int32, shape, 0) <= lax.broadcasted_iota(jnp.int32, shape, 1)
     tri = upto.astype(f32).astype(bf)
+    both_shape = (2 * BLOCK, 2 * BLOCK)
+    from_at, to_at = (lax.broadcasted_iota(jnp.int32, both_shape, i) for i in range(2))
+    tri_both = ((from_at <= to_at) & ((from_at < BLOCK) == (to_at < BLOCK))).astype(f32).astype(bf)
     centre = BLOCK // 2
     eye = lax.broadcasted_iota(jnp.int32, (groups, BLOCK), 0) == lax.broadcasted_iota(
         jnp.int32, (groups, BLOCK), 1
@@ -527,9 +560,9 @@
             + jnp.dot(low2, tri, preferred_element_type=f32)
         )
         middle = level[:, centre : centre + 1]
-        lifts[b] = jnp.exp(middle - level)
+        lifts[:, b * BLOCK : (b + 1) * BLOCK] = jnp.exp(middle - level)
         grown = jnp.exp(level - middle)
-        grows[b] = grown
+        grows[:, b * BLOCK : (b + 1) * BLOCK] = grown
         begins.append(across(jnp.exp(middle)))
         lasts.append(across(grown[:, BLOCK - 1 :]))
     rates, turns = columns_of
@@ -551,29 +584,50 @@
     whole = times(reach, end)
 
     pump(2)
-
-    @pl.when(fast)
-    def _():
-        for c in query_weights:
-            c.start()
-
-    sent.extend(query_weights)
-    with jax.named_scope("ssm_wait"):
-        spread_done(0)
-    with jax.named_scope("project_u"):
-        total_in[...] += part_of(w_ssm, 1 - late)
-        give_u[...] = total_in[:, mine_at(1 - par)].astype(bf)
-    launch(remote(give_u, got_u, g_s.at[0], g_r.at[0], sp=pair))
+    narrow = wide // 2
+
+    def state_inputs(h):
+        with jax.named_scope("ssm_wait"):
+            spread_done(0, (2 * h, 2 * h + 1))
+        with jax.named_scope("project_u"):
+            for e in range(2):
+                lanes = slice(e * wide + h * narrow, e * wide + (h + 1) * narrow)
+                total_in[:, lanes] += jnp.dot(
+                    normed[1 - late], w_ssm[1 - late, :, lanes], preferred_element_type=f32
+                )
+            give_u[h] = total_in[:, half_at(1 - par, h)].astype(bf)
+        launch(remote(give_u.at[h], got_u.at[h], g_s.at[3 * h], g_r.at[3 * h], sp=pair))
+
+    def half_at(e, h):
+        return pl.ds(pl.multiple_of(e * wide + h * narrow, 128), narrow)
+
+    def turn_inputs(h):
+        with jax.named_scope("got_u"):
+            remote(got_u.at[h], got_u.at[h], g_s.at[3 * h], g_r.at[3 * h], sp=pair).wait_recv()
+        with jax.named_scope("turn_u"):
+            u = total_in[:, half_at(par, h)] + got_u[h].astype(f32)
+            u_scr[h * narrow : (h + 1) * narrow, :] = jnp.transpose(u.astype(bf).astype(f32))
+
+    state_inputs(0)
+    state_inputs(1)
+    launch_if(slow, out_weights)
     pump(2)
-    for c in range(2):
-        launch(over_z(4, c))
-    def query_parts():
+    turn_inputs(0)
+    launch_if(fast, out_weights)
+    launch_if(slow, attend_weights)
+
+    def query_parts(h):
         with jax.named_scope("query_wait"):
-            spread_done(1)
+            spread_done(1, (2 * h, 2 * h + 1))
         with jax.named_scope("project_q"):
-            total_in[...] = part_of(w_query, 0) + part_of(w_query, 1)
-            give_q[...] = total_in[:, mine_at(1 - par)].astype(bf)
-        launch(remote(give_q, got_q, g_s.at[1], g_r.at[1], sp=pair))
+            for e in range(2):
+                lanes = slice(e * wide + h * narrow, e * wide + (h + 1) * narrow)
+                total_q[:, lanes] = sum(
+                    jnp.dot(normed[slot], w_query[slot, :, lanes], preferred_element_type=f32)
+                    for slot in range(2)
+                )
+            give_q[h] = total_q[:, half_at(1 - par, h)].astype(bf)
+        launch(remote(give_q.at[h], got_q.at[h], g_s.at[1 + 3 * h], g_r.at[1 + 3 * h], sp=pair))
 
     def key_parts():
         with jax.named_scope("key_wait"):
@@ -590,13 +644,6 @@
 
         return jnp.where(par == 0, both[0], both[1])
 
-    own_kv = key_parts()
-    with jax.named_scope("got_u"):
-        remote(got_u, got_u, g_s.at[0], g_r.at[0], sp=pair).wait_recv()
-    with jax.named_scope("turn_u"):
-        u = total_in[:, mine_at(par)] + got_u[...].astype(f32)
-        u_scr[...] = jnp.transpose(u.astype(bf).astype(f32))
-
     tail = kv_scr.at[pl.ds(2 * WINDOW, WINDOW)]
     head = kv_scr.at[pl.ds(0, WINDOW)]
     hand_kv = remote(tail, head, p_s.at[5], p_r.at[5], sp=across_z)
@@ -615,28 +662,35 @@
     lane = lax.broadcasted_iota(jnp.int32, (state, BLOCK), 1)
     ends = [jnp.zeros((state, BLOCK), f32)] * 4
     for g in range(groups):
+        if g == groups // 2:
+            turn_inputs(1)
+            launch_if(fast, attend_weights)
         with jax.named_scope("first"):
             u = u_scr[g * GROUP_CH : (g + 1) * GROUP_CH, :]
             drive = jnp.dot(inm[g], u.astype(bf), preferred_element_type=f32)
-            up_re, up_im = tab[g, 0], tab[g, 1]
-            lifted = []
-            for b in range(2):
-                span = slice(b * BLOCK, (b + 1) * BLOCK)
-                row = lifts[b, g : g + 1, :]
-                d_re, d_im = drive[:state, span] * row, drive[state:, span] * row
-                lifted += [d_re * up_re - d_im * up_im, d_re * up_im + d_im * up_re]
-            sums = split_dot(jnp.concatenate(lifted, axis=0), tri)
+            up_re = jnp.concatenate([tab[g, 0]] * 2, axis=1)
+            up_im = jnp.concatenate([tab[g, 1]] * 2, axis=1)
+            row = lifts[g : g + 1, :]
+            d_re, d_im = drive[:state] * row, drive[state:] * row
+            lifted = jnp.concatenate([d_re * up_re - d_im * up_im, d_re * up_im + d_im * up_re], axis=0)
+            sums = jnp.dot(lifted.astype(bf), tri_both, preferred_element_type=f32)
             prefix[g] = sums
             ends = [
-                jnp.where(lane == g, sums[i * state : (i + 1) * state, BLOCK - 1 :], ends[i])
+                jnp.where(
+                    lane == g,
+                    sums[i % 2 * state : (i % 2 + 1) * state, (i // 2 + 1) * BLOCK - 1 : (i // 2 + 1) * BLOCK],
+                    ends[i],
+                )
                 for i in range(4)
             ]
         if g == 5:
-            settle_kv()
-        if g == 9:
-            query_parts()
-        if g in (11, 14):
+            own_kv = key_parts()
+        if g in (1, 3, 9):
             pump(1)
+        if g == 11:
+            query_parts(0)
+            if False:
+                pump(1)
     with jax.named_scope("carry"):
         own = [scaled(lasts[b], times(end, (ends[2 * b], ends[2 * b + 1]))) for b in range(2)]
         decay = [scaled(lasts[b] * begins[b], whole) for b in range(2)]
@@ -648,47 +702,15 @@
         hand_state.start()
         carry_in[...] = jnp.zeros(carry_in.shape, f32)
 
-    for c in range(2):
-        launch(over_z(3, c))
-    with jax.named_scope("q_wait"):
-        remote(got_q, got_q, g_s.at[1], g_r.at[1], sp=pair).wait_recv()
-    q_scr[...] = (total_in[:, mine_at(par)] + got_q[...].astype(f32)).astype(bf)
-    gap_shape = (WINDOW, 2 * WINDOW)
-    at = lax.broadcasted_iota(jnp.int32, gap_shape, 1)
-    gap = lax.broadcasted_iota(jnp.int32, gap_shape, 0) + WINDOW - at
-    inside = (gap >= 0) & (gap < WINDOW)
-    inside_first = inside & (at >= WINDOW * (1 - late))
-    sink_lane = lax.broadcasted_iota(jnp.int32, sinks.shape, 1)
-    for b in (1, 0):
-        if b == 0:
-
-            @pl.when(late == 1)
-            def _():
-                with jax.named_scope("hand_wait"):
-                    hand_kv.wait_recv()
-                    hand_state.wait_recv()
-
-        keys = kv_scr[b * WINDOW : (b + 2) * WINDOW, :HEAD_DIM]
-        values = kv_scr[b * WINDOW : (b + 2) * WINDOW, HEAD_DIM:]
-        valid = inside if b else inside_first
-        outs = []
-        for h in range(heads):
-            with jax.named_scope("head"):
-                q = q_scr[b * WINDOW : (b + 1) * WINDOW, h * HEAD_DIM : (h + 1) * HEAD_DIM]
-                scores = lax.dot_general(q, keys, (((1,), (1,)), ((), ())), preferred_element_type=f32)
-                scores = jnp.where(valid, scores * HEAD_DIM ** (-0.5), floor_score)
-                sink = jnp.sum(jnp.where(sink_lane == par * heads + h, sinks[...], 0.0), axis=1, keepdims=True)
-                peak = jnp.maximum(jnp.max(scores, axis=1, keepdims=True), sink)
-                raised = jnp.where(valid, jnp.exp(scores - peak), 0.0)
-                total = jnp.sum(raised, axis=1, keepdims=True) + jnp.exp(sink - peak)
-                weights = (raised / total).astype(bf)
-                outs.append(jnp.dot(weights, values, preferred_element_type=f32))
-            if h == 2 and b == 0:
-                pump(1)
-        act_a[par, b * BLOCK : (b + 1) * BLOCK, :] = jnp.concatenate(outs, axis=1).astype(bf)
-
-    mix_a = remote(act_a.at[par], act_a.at[par], e_s.at[4], e_r.at[4], sp=pair)
-    launch(mix_a)
+    query_parts(1)
+    settle_kv()
+    pump(1)
+
+    @pl.when(late == 1)
+    def _():
+        with jax.named_scope("hand_state"):
+            hand_state.wait_recv()
+
     back = jnp.transpose(carry_in[...])
     entry = (back[:state], back[state:])
 
@@ -707,53 +729,95 @@
     for g in range(groups):
         with jax.named_scope("second"):
             u = u_scr[g * GROUP_CH : (g + 1) * GROUP_CH, :]
-            down = (tab[g, 2], tab[g, 3])
+            down = [jnp.concatenate([tab[g, i]] * 2, axis=1) for i in (2, 3)]
             chosen = lax.broadcasted_iota(jnp.int32, skip.shape, 1) == first + g
             skips = jnp.sum(jnp.where(chosen, skip[...], 0.0), axis=1, keepdims=True)
-            states = []
-            for b in range(2):
-                at_re = slice(2 * b * state, (2 * b + 1) * state)
-                at_im = slice((2 * b + 1) * state, (2 * b + 2) * state)
-                p = (prefix[g, at_re] + base[b][0][:, g : g + 1], prefix[g, at_im] + base[b][1][:, g : g + 1])
-                states.append(jnp.concatenate(scaled(grows[b, g : g + 1, :], times(down, p)), axis=0))
-            high, low = halves(jnp.concatenate(states, axis=1))
-            y = jnp.dot(read[g], high, preferred_element_type=f32) + jnp.dot(
-                read[g], low, preferred_element_type=f32
-            )
+            p = [
+                prefix[g, i * state : (i + 1) * state]
+                + jnp.concatenate(
+                    [jnp.broadcast_to(base[b][i][:, g : g + 1], (state, BLOCK)) for b in range(2)], axis=1
+                )
+                for i in range(2)
+            ]
+            states = jnp.concatenate(scaled(grows[g : g + 1, :], times(down, p)), axis=0).astype(bf)
+            y = jnp.dot(read[g], states, preferred_element_type=f32)
             y_scr[g * GROUP_CH : (g + 1) * GROUP_CH, :] = y + skips * u
-        if g == 7:
-            pump(1)
         if (g + 1) % (groups // 2) == 0:
             side = (g + 1) // (groups // 2) - 1
             lanes = slice(side * BLOCK, (side + 1) * BLOCK)
             with jax.named_scope("gelu"):
                 act_s[par, :, lanes] = jnp.transpose(jax.nn.gelu(y_scr[lanes, :])).astype(bf)
             half_s = act_s.at[par, :, pl.ds(side * BLOCK, BLOCK)]
-            launch(remote(half_s, half_s, e_s.at[5 + side], e_r.at[5 + side], sp=pair))
+            launch(remote(half_s, half_s, e_s.at[6 + side], e_r.at[6 + side], sp=pair))
+
+    gap_shape = (WINDOW, 2 * WINDOW)
+    at = lax.broadcasted_iota(jnp.int32, gap_shape, 1)
+    gap = lax.broadcasted_iota(jnp.int32, gap_shape, 0) + WINDOW - at
+    inside = (gap >= 0) & (gap < WINDOW)
+    inside_first = inside & (at >= WINDOW * (1 - late))
+    sink_lane = lax.broadcasted_iota(jnp.int32, sinks.shape, 1)
+    pump(1)
+    for side in range(2):
+        pump(1)
+        with jax.named_scope("q_wait"):
+            remote(got_q.at[side], got_q.at[side], g_s.at[1 + 3 * side], g_r.at[1 + 3 * side], sp=pair).wait_recv()
+        q_scr[:, side * narrow : (side + 1) * narrow] = (
+            (total_q[:, half_at(par, side)] + got_q[side].astype(f32)) * HEAD_DIM ** (-0.5)
+        ).astype(bf)
+        for b in (1, 0):
+            if b == 0 and side == 0:
+
+                @pl.when(late == 1)
+                def _():
+                    with jax.named_scope("hand_kv"):
+                        hand_kv.wait_recv()
+
+            keys = kv_scr[b * WINDOW : (b + 2) * WINDOW, :HEAD_DIM]
+            values = kv_scr[b * WINDOW : (b + 2) * WINDOW, HEAD_DIM:]
+            valid = inside if b else inside_first
+            outs = []
+            for h in range(side * heads // 2, (side + 1) * heads // 2):
+                with jax.named_scope("head"):
+                    q = q_scr[b * WINDOW : (b + 1) * WINDOW, h * HEAD_DIM : (h + 1) * HEAD_DIM]
+                    scores = lax.dot_general(q, keys, (((1,), (1,)), ((), ())), preferred_element_type=f32)
+                    scores = jnp.where(valid, scores, floor_score)
+                    sink = jnp.sum(
+                        jnp.where(sink_lane == par * heads + h, sinks[...], 0.0), axis=1, keepdims=True
+                    )
+                    peak = jnp.maximum(jnp.max(scores, axis=1, keepdims=True), sink)
+                    raised = jnp.exp(scores - peak)
+                    total = jnp.sum(raised, axis=1, keepdims=True) + jnp.exp(sink - peak)
+                    weights = (raised * (1.0 / total)).astype(bf)
+                    outs.append(jnp.dot(weights, values, preferred_element_type=f32))
+            act_a[par, b * BLOCK : (b + 1) * BLOCK, side * narrow : (side + 1) * narrow] = jnp.concatenate(
+                outs, axis=1
+            ).astype(bf)
+        half_a = act_a.at[par, :, pl.ds(side * narrow, narrow)]
+        launch(remote(half_a, half_a, e_s.at[4 + side], e_r.at[4 + side], sp=pair))
 
     size, chunk = tokens // 2, cols // 2
-    theirs = act_a.at[1 - par]
-    with jax.named_scope("mix_a"):
-        remote(theirs, theirs, e_s.at[4], e_r.at[4], sp=pair).wait_recv()
-    pump(len(queue))
-
-    def attend_part(slot):
+    def state_part(slot):
         for side in range(2):
             lanes = slice(side * chunk, (side + 1) * chunk)
-            rows_a = [jnp.dot(act_a[e], wo_a[slot, e * wide : (e + 1) * wide, lanes], preferred_element_type=f32)
-                      for e in range(2)]
-            pa[slot, :, lanes] = rows_a[0] + rows_a[1]
-
-    with jax.named_scope("attend"):
-        attend_part(late)
-    with jax.named_scope("out_wait"):
-        spread_done(4)
-    with jax.named_scope("attend"):
-        attend_part(1 - late)
+            both = [jnp.dot(act_s[e], wo_s[slot, e * wide : (e + 1) * wide, lanes], preferred_element_type=f32)
+                    for e in range(2)]
+            pa[slot, :, lanes] = both[0] + both[1]
+
     with jax.named_scope("mix_s"):
         for side in range(2):
             theirs = act_s.at[1 - par, :, pl.ds(side * BLOCK, BLOCK)]
-            remote(theirs, theirs, e_s.at[5 + side], e_r.at[5 + side], sp=pair).wait_recv()
+            remote(theirs, theirs, e_s.at[6 + side], e_r.at[6 + side], sp=pair).wait_recv()
+    with jax.named_scope("state"):
+        state_part(late)
+    pump(len(queue))
+    with jax.named_scope("out_wait"):
+        spread_done(3)
+    with jax.named_scope("state"):
+        state_part(1 - late)
+    with jax.named_scope("mix_a"):
+        for side in range(2):
+            theirs = act_a.at[1 - par, :, pl.ds(side * narrow, narrow)]
+            remote(theirs, theirs, e_s.at[4 + side], e_r.at[4 + side], sp=pair).wait_recv()
 
     def target(who, i):
         first_column = lax.rem(who + 2 * (i // 2), n) * cols + (i % 2) * chunk
@@ -764,7 +828,7 @@
         total = pa[slot, :, lanes]
         for e in range(2):
             total = total + jnp.dot(
-                act_s[e], wo_s[slot, e * wide : (e + 1) * wide, lanes], preferred_element_type=f32
+                act_a[e], wo_a[slot, e * wide : (e + 1) * wide, lanes], preferred_element_type=f32
             )
         for e in range(2):
             for side in range(2):
@@ -783,7 +847,7 @@
     for i in range(4):
         if i == 2:
             with jax.named_scope("out_wait"):
-                spread_done(3)
+                spread_done(4)
         with jax.named_scope("multiply"):
             multiply(i)
         if i:
@@ -831,20 +895,20 @@
             vm(parts.shape, bf), vm(reads.shape, bf), vm(skip.shape, f32),
             vm((groups, length), f32), vm(sinks.shape, f32),
             vm((groups, 4, state, BLOCK), f32), vm((groups, 2 * state, GROUP_CH), bf),
-            vm((groups, GROUP_CH, 2 * state), bf), vm((2, groups, BLOCK), f32), vm((2, groups, BLOCK), f32),
-            vm((groups, 4 * state, BLOCK), f32), vm((wide, length), f32), vm((length, wide), bf),
+            vm((groups, GROUP_CH, 2 * state), bf), vm((groups, length), f32), vm((groups, length), f32),
+            vm((groups, 2 * state, length), f32), vm((wide, length), f32), vm((length, wide), bf),
             vm((length + WINDOW, 2 * HEAD_DIM), bf), vm((wide, length), f32),
             vm((2, length, wide), bf), vm((2, length, wide), bf),
             vm((groups, 2 * state), f32), vm((groups, 2 * state), f32),
-            vm((8, tokens), f32), vm((8, tokens), f32), vm((length, 2 * wide), f32),
-            vm((length, wide), bf), vm((length, wide), bf), vm((length, 2 * HEAD_DIM), bf),
-            vm((length, wide), bf), vm((length, wide), bf), vm((length, 2 * HEAD_DIM), bf),
+            vm((8, tokens), f32), vm((8, tokens), f32), vm((length, 2 * wide), f32), vm((length, 2 * wide), f32),
+            vm((2, length, wide // 2), bf), vm((2, length, wide // 2), bf), vm((length, 2 * HEAD_DIM), bf),
+            vm((2, length, wide // 2), bf), vm((2, length, wide // 2), bf), vm((length, 2 * HEAD_DIM), bf),
             vm((2, length, cols), f32),
             vm((4, 2, 2, tokens // 2, cols // 2), f32), vm((4, 2, 2, tokens // 2, cols // 2), bf),
             vm((4, 2, tokens // 2, cols // 2), bf), vm((4, tokens // 2, cols // 2), bf),
             vm((4, tokens // 2, cols // 2), bf),
             dma((15,)), dma((5, 4)), dma((5, 4)), dma((7,)), dma((7,)), dma((5, 4, 3)), dma((5, 4, 3)),
-            dma((3,)), dma((3,)), dma((4,)), dma((4,)), dma((7,)), dma((7,)), dma((4,)),
+            dma((5,)), dma((5,)), dma((4,)), dma((4,)), dma((8,)), dma((8,)), dma((4,)),
         ],
         compiler_params=pltpu.CompilerParams(collective_id=0, has_side_effects=True),
     )(x, gain, ssm, query, key, value, rate, turn, parts, reads, skip, shift, sinks, ows, owa)

time: 55.8 us -> 50.3 us (0.901)
  Pallas kernels: 53.9 us -> 48.4 us
    pallas_call x1, Pallas kernels: 53.9 us -> 48.4 us  [layer(): pl.pallas_call(layer_kernel, out_shape=jax.ShapeDtypeStruct((tokens // 2,...]
where the time goes in v3:
time: 50.3 us; the launch traced here: 50.1 us
  Pallas kernels  48.4 us (96%)
  local copies, waits for them, and re-layouts  1.67 us (3%)
    pallas_call x1, Pallas kernels, layer(): pl.pallas_call(layer_kernel, out_shape=jax.ShapeDtypeStruct((tokens // 2,...  48.4 us
    unnamed x1, local copies, waits for them, and re-layouts  1.67 us

profile of v3, /device:TPU:0, one launch (start us, length us, event | category | flops | bytes accessed | tf_op | source)
XLA Modules:
  0.0 50.1 jit_solution(2546854635401865707)
XLA Ops:
  0.0 48.4 %shard_map.145 = bf16[64,2048]{1,0:T(8,128)(2,1)} custom-call(bf16[128,1024]{1,0:T(8,128)(2,1)} %x_in.1, f32[1,2048]{1,0:T(1,128)} %bitcast.7, bf16[512,512]{1,0:T(8,128)(2,1)} %ssm.1, bf16[512,512]{1,0:T(8,128)(2,1)} %query.1, bf16[512,128]{1,0:T(8,128)(2,1)} %key_in.1, bf16[512,128]{1,0:T(8,128)(2,1)} %value_in.1, f32[32,64]{1,0:T(8,128)} %rate_in.1, ...), custom_call_target="tpu_custom_call" | custom-call | tf_op jit(solution)/shard_map/pallas_call | solution.py:885
  48.4 1.7 %copy.17 = bf16[64,2048]{1,0:T(8,128)(2,1)} copy(bf16[64,2048]{1,0:T(8,128)(2,1)} %shard_map.145) | data formatting | bytes 524288

commit v4 on v3

--- a/solution.py
+++ b/solution.py
@@ -336,7 +336,7 @@
     part = rows // n_fs
     into = (w_ssm, w_query, None, wo_s, wo_a)
     origin = (ssm, query, None, ows, owa)
-    cuts = (4, 4, 2, 2, 2)
+    cuts = (4, 4, 2, 2, 4)
 
     def stripe(c):
         return pl.ds(c % 2 * wide + c // 2 * (wide // 2), wide // 2)
@@ -454,7 +454,7 @@
     at_end = k * (n - 1 - k) == 0
     sides = pl.ds(pl.multiple_of(t * half, 128), half)
     launch(remote(x_in, xf.at[:, sides], p_s.at[0], p_r.at[0], tp=other))
-    slow, fast = t == 0, t == 1
+    slow, fast, at_mid = t == 0, t == 1, k * (n - 1 - k) > 0
 
     def launch_if(choice, copies):
         @pl.when(choice)
@@ -466,12 +466,12 @@
     early_keys = [over_z(2, c) for c in range(2)]
     query_weights = [over_z(1, c) for c in range(cuts[1])]
     out_weights = [over_z(3, c) for c in range(2)]
-    attend_weights = [over_z(4, c) for c in range(2)]
+    attend_weights = [over_z(4, c) for c in range(cuts[4])]
     give_x = remote(x_in.at[:, pl.ds(pl.multiple_of((1 - par) * rows, 128), rows)], xp.at[t],
                     p_s.at[1], p_r.at[1], sp=pair)
+    launch(remote(shift_rows(1 - par), shift_at(par), p_s.at[2], p_r.at[2], sp=pair))
     state_weights[0].start()
     launch_if(slow, state_weights[1:])
-    launch(remote(shift_rows(1 - par), shift_at(par), p_s.at[2], p_r.at[2], sp=pair))
     launch_if(slow | jnp.logical_not(at_end), [give_x])
     launch_if(slow, early_keys)
     sent.extend(state_weights + early_keys + query_weights + out_weights + attend_weights + [give_x])
@@ -497,7 +497,7 @@
         )
         line = jnp.sum(jnp.where(same, scale, 0.0), axis=0, keepdims=True)
         scale_out[...] = jnp.broadcast_to(line, scale_out.shape)
-    launch_if(fast, state_weights[1:])
+    launch_if(fast, state_weights[1:] + early_keys)
     launch_if(fast & at_end, [give_x])
     launch(remote(scale_out, scale_in, p_s.at[3], p_r.at[3], sp=pair))
     with jax.named_scope("norm"):
@@ -506,32 +506,20 @@
             normed[slot, own_rows] = (block * scale * gain_of(slot)).astype(bf)
     with jax.named_scope("tables"):
         columns_of = lax.fori_loop(10, groups, tables, columns_of)
+    hand_x = remote(xp.at[t], xp.at[t], p_s.at[4], p_r.at[4], tp=other)
+    sent.append(hand_x)
+
+    def take_x():
+        with jax.named_scope("next_x"):
+            remote(xp.at[t], xp.at[t], p_s.at[1], p_r.at[1], sp=pair).wait_recv()
+        hand_x.start()
+
+    pump(1)
+    pl.when(at_end)(take_x)
+    pump(1)
     pump(2)
-    launch_if(fast, early_keys)
-    launch_if(slow, query_weights)
-    pump(2)
-    launch_if(fast, query_weights)
-    with jax.named_scope("next_x"):
-        remote(xp.at[t], xp.at[t], p_s.at[1], p_r.at[1], sp=pair).wait_recv()
-    launch(remote(xp.at[t], xp.at[t], p_s.at[4], p_r.at[4], tp=other))
-    with jax.named_scope("partner_x"):
-        remote(xp.at[other], xp.at[other], p_s.at[4], p_r.at[4], tp=other).wait_recv()
-        remote(scale_in, scale_in, p_s.at[3], p_r.at[3], sp=pair).wait_recv()
-    with jax.named_scope("norm"):
-        scale = column(scale_in[0:1, :])
-        for slot in range(2):
-            normed[slot, pair_rows] = (xp[slot].astype(f32) * scale * gain_of(slot)).astype(bf)
-    for c in local[9:]:
-        c.wait()
-    with jax.named_scope("own_u"):
-        total_in[...] = jnp.dot(normed[late], w_ssm[late], preferred_element_type=f32)
-
-    def part_of(w, slot):
-        return jnp.dot(normed[slot], w[slot], preferred_element_type=f32)
-
-    def mine_at(e):
-        return pl.ds(pl.multiple_of(e * wide, 128), wide)
-
+    for c in query_weights:
+        c.start()
     near_shift = shift_at(1 - par)
     remote(near_shift, near_shift, p_s.at[2], p_r.at[2], sp=pair).wait_recv()
 
@@ -583,7 +571,26 @@
     reach, end = spiral(centre + 1.0), spiral(BLOCK - 1.0 - centre)
     whole = times(reach, end)
 
-    pump(2)
+    pl.when(at_mid)(take_x)
+    with jax.named_scope("partner_x"):
+        remote(xp.at[other], xp.at[other], p_s.at[4], p_r.at[4], tp=other).wait_recv()
+        remote(scale_in, scale_in, p_s.at[3], p_r.at[3], sp=pair).wait_recv()
+    with jax.named_scope("norm"):
+        scale = column(scale_in[0:1, :])
+        for slot in range(2):
+            normed[slot, pair_rows] = (xp[slot].astype(f32) * scale * gain_of(slot)).astype(bf)
+    for c in local[9:]:
+        c.wait()
+    with jax.named_scope("own_u"):
+        total_in[...] = jnp.dot(normed[late], w_ssm[late], preferred_element_type=f32)
+
+    def part_of(w, slot):
+        return jnp.dot(normed[slot], w[slot], preferred_element_type=f32)
+
+    def mine_at(e):
+        return pl.ds(pl.multiple_of(e * wide, 128), wide)
+
+
     narrow = wide // 2
 
     def state_inputs(h):
@@ -609,7 +616,9 @@
             u_scr[h * narrow : (h + 1) * narrow, :] = jnp.transpose(u.astype(bf).astype(f32))
 
     state_inputs(0)
+    pump(1)
     state_inputs(1)
+    pump(1)
     launch_if(slow, out_weights)
     pump(2)
     turn_inputs(0)
@@ -685,10 +694,11 @@
             ]
         if g == 5:
             own_kv = key_parts()
-        if g in (1, 3, 9):
+        if g in (1, 3):
             pump(1)
         if g == 11:
             query_parts(0)
+            pump(1)
             if False:
                 pump(1)
     with jax.named_scope("carry"):
@@ -756,7 +766,7 @@
     inside = (gap >= 0) & (gap < WINDOW)
     inside_first = inside & (at >= WINDOW * (1 - late))
     sink_lane = lax.broadcasted_iota(jnp.int32, sinks.shape, 1)
-    pump(1)
+    pump(2)
     for side in range(2):
         pump(1)
         with jax.named_scope("q_wait"):

time: 50.3 us -> 49.4 us (0.982)
  Pallas kernels: 48.4 us -> 47.5 us
    pallas_call x1, Pallas kernels: 48.4 us -> 47.5 us  [layer(): pl.pallas_call(layer_kernel, out_shape=jax.ShapeDtypeStruct((tokens // 2,...]
where the time goes in v4:
time: 49.4 us; the launch traced here: 49.2 us
  Pallas kernels  47.5 us (96%)
  local copies, waits for them, and re-layouts  1.67 us (3%)
    pallas_call x1, Pallas kernels, layer(): pl.pallas_call(layer_kernel, out_shape=jax.ShapeDtypeStruct((tokens // 2,...  47.5 us
    unnamed x1, local copies, waits for them, and re-layouts  1.67 us

profile of v4, /device:TPU:0, one launch (start us, length us, event | category | flops | bytes accessed | tf_op | source)
XLA Modules:
  0.0 49.2 jit_solution(2096879522508658045)
XLA Ops:
  0.0 47.5 %shard_map.145 = bf16[64,2048]{1,0:T(8,128)(2,1)} custom-call(bf16[128,1024]{1,0:T(8,128)(2,1)} %x_in.1, f32[1,2048]{1,0:T(1,128)} %bitcast.7, bf16[512,512]{1,0:T(8,128)(2,1)} %ssm.1, bf16[512,512]{1,0:T(8,128)(2,1)} %query.1, bf16[512,128]{1,0:T(8,128)(2,1)} %key_in.1, bf16[512,128]{1,0:T(8,128)(2,1)} %value_in.1, f32[32,64]{1,0:T(8,128)} %rate_in.1, ...), custom_call_target="tpu_custom_call" | custom-call | tf_op jit(solution)/shard_map/pallas_call | solution.py:895
  47.5 1.7 %copy.17 = bf16[64,2048]{1,0:T(8,128)(2,1)} copy(bf16[64,2048]{1,0:T(8,128)(2,1)} %shard_map.145) | data formatting | bytes 524288

commit v5 on v4

--- a/solution.py
+++ b/solution.py
@@ -318,7 +318,7 @@
                  parts, reads, skip, shift, sinks, tab, inm, read, lifts, grows, prefix, u_scr, q_scr,
                  kv_scr, y_scr, act_s, act_a, carry_out, carry_in, scale_out, scale_in, total_in, total_q,
                  give_u, give_q, give_kv, got_u, got_q, got_kv, pa, pf, pb, got, fsend, res,
-                 loc, z_s, z_r, p_s, p_r, x_s, x_r, g_s, g_r, d_s, d_r, e_s, e_r, o_s):
+                 loc, z_s, z_r, p_s, p_r, x_s, x_r, g_r, d_s, d_r, e_r, o_s):
     f32, bf = jnp.float32, jnp.bfloat16
     k, f, t = lax.axis_index("sp"), lax.axis_index("fs"), lax.axis_index("tp")
     n, n_fs = 4, 4
@@ -337,6 +337,7 @@
     into = (w_ssm, w_query, None, wo_s, wo_a)
     origin = (ssm, query, None, ows, owa)
     cuts = (4, 4, 2, 2, 4)
+    at_piece = [sum(cuts[:w]) for w in range(5)]
 
     def stripe(c):
         return pl.ds(c % 2 * wide + c // 2 * (wide // 2), wide // 2)
@@ -357,21 +358,30 @@
         else:
             size = part // cuts[w]
             source = origin[w].at[pl.ds(pl.multiple_of(f * part + c * size, 16), size)]
-        return remote(source, region(w, c, f, late), z_s.at[w, c], z_r.at[w, c], sp=across_z)
+        return remote(source, region(w, c, f, late), z_s.at[at_piece[w] + c], z_r.at[at_piece[w] + c], sp=across_z)
 
     def spread_here(w, c):
         block = region(w, c, f, 1 - late)
-        remote(block, block, z_s.at[w, c], z_r.at[w, c], sp=across_z).wait_recv()
-        for i, who in enumerate((far, fx, fy)):
-            launch(remote(block, block, x_s.at[w, c, i], x_r.at[w, c, i], fs=who))
+        remote(block, block, z_s.at[at_piece[w] + c], z_r.at[at_piece[w] + c], sp=across_z).wait_recv()
+        slot = len(spreads) % 4
+        if len(spreads) >= 4:
+            for copy in spreads[-4]:
+                copy.wait_send()
+        spreads.append([
+            remote(block, block, x_s.at[slot, i], x_r.at[at_piece[w] + c, i], fs=who)
+            for i, who in enumerate((far, fx, fy))
+        ])
+        for copy in spreads[-1]:
+            copy.start()
 
     def spread_done(w, pieces=None):
         for c in pieces or range(cuts[w]):
             for i, who in enumerate((far, fx, fy)):
                 block = region(w, c, who, 1 - late)
-                remote(block, block, x_s.at[w, c, i], x_r.at[w, c, i], fs=who).wait_recv()
-
-    sent = []
+                remote(block, block, x_s.at[0, i], x_r.at[at_piece[w] + c, i], fs=who).wait_recv()
+
+    sent, spreads = [], []
+    g_s, e_s = [loc.at[i] for i in range(5)], [loc.at[5 + i] for i in range(8)]
 
     def launch(c):
         c.start()
@@ -603,14 +613,14 @@
                     normed[1 - late], w_ssm[1 - late, :, lanes], preferred_element_type=f32
                 )
             give_u[h] = total_in[:, half_at(1 - par, h)].astype(bf)
-        launch(remote(give_u.at[h], got_u.at[h], g_s.at[3 * h], g_r.at[3 * h], sp=pair))
+        launch(remote(give_u.at[h], got_u.at[h], g_s[3 * h], g_r.at[3 * h], sp=pair))
 
     def half_at(e, h):
         return pl.ds(pl.multiple_of(e * wide + h * narrow, 128), narrow)
 
     def turn_inputs(h):
         with jax.named_scope("got_u"):
-            remote(got_u.at[h], got_u.at[h], g_s.at[3 * h], g_r.at[3 * h], sp=pair).wait_recv()
+            remote(got_u.at[h], got_u.at[h], g_s[3 * h], g_r.at[3 * h], sp=pair).wait_recv()
         with jax.named_scope("turn_u"):
             u = total_in[:, half_at(par, h)] + got_u[h].astype(f32)
             u_scr[h * narrow : (h + 1) * narrow, :] = jnp.transpose(u.astype(bf).astype(f32))
@@ -636,7 +646,7 @@
                     for slot in range(2)
                 )
             give_q[h] = total_q[:, half_at(1 - par, h)].astype(bf)
-        launch(remote(give_q.at[h], got_q.at[h], g_s.at[1 + 3 * h], g_r.at[1 + 3 * h], sp=pair))
+        launch(remote(give_q.at[h], got_q.at[h], g_s[1 + 3 * h], g_r.at[1 + 3 * h], sp=pair))
 
     def key_parts():
         with jax.named_scope("key_wait"):
@@ -649,7 +659,7 @@
                 for e in range(2)
             ]
             give_kv[...] = jnp.where(par == 0, both[1], both[0]).astype(bf)
-        launch(remote(give_kv, got_kv, g_s.at[2], g_r.at[2], sp=pair))
+        launch(remote(give_kv, got_kv, g_s[2], g_r.at[2], sp=pair))
 
         return jnp.where(par == 0, both[0], both[1])
 
@@ -660,7 +670,7 @@
 
     def settle_kv():
         with jax.named_scope("kv_wait"):
-            remote(got_kv, got_kv, g_s.at[2], g_r.at[2], sp=pair).wait_recv()
+            remote(got_kv, got_kv, g_s[2], g_r.at[2], sp=pair).wait_recv()
         kv_scr[WINDOW:, :] = (own_kv + got_kv[...].astype(f32)).astype(bf)
 
         @pl.when(late == 0)
@@ -758,7 +768,7 @@
             with jax.named_scope("gelu"):
                 act_s[par, :, lanes] = jnp.transpose(jax.nn.gelu(y_scr[lanes, :])).astype(bf)
             half_s = act_s.at[par, :, pl.ds(side * BLOCK, BLOCK)]
-            launch(remote(half_s, half_s, e_s.at[6 + side], e_r.at[6 + side], sp=pair))
+            launch(remote(half_s, half_s, e_s[6 + side], e_r.at[6 + side], sp=pair))
 
     gap_shape = (WINDOW, 2 * WINDOW)
     at = lax.broadcasted_iota(jnp.int32, gap_shape, 1)
@@ -770,7 +780,7 @@
     for side in range(2):
         pump(1)
         with jax.named_scope("q_wait"):
-            remote(got_q.at[side], got_q.at[side], g_s.at[1 + 3 * side], g_r.at[1 + 3 * side], sp=pair).wait_recv()
+            remote(got_q.at[side], got_q.at[side], g_s[1 + 3 * side], g_r.at[1 + 3 * side], sp=pair).wait_recv()
         q_scr[:, side * narrow : (side + 1) * narrow] = (
             (total_q[:, half_at(par, side)] + got_q[side].astype(f32)) * HEAD_DIM ** (-0.5)
         ).astype(bf)
@@ -803,7 +813,7 @@
                 outs, axis=1
             ).astype(bf)
         half_a = act_a.at[par, :, pl.ds(side * narrow, narrow)]
-        launch(remote(half_a, half_a, e_s.at[4 + side], e_r.at[4 + side], sp=pair))
+        launch(remote(half_a, half_a, e_s[4 + side], e_r.at[4 + side], sp=pair))
 
     size, chunk = tokens // 2, cols // 2
     def state_part(slot):
@@ -816,7 +826,7 @@
     with jax.named_scope("mix_s"):
         for side in range(2):
             theirs = act_s.at[1 - par, :, pl.ds(side * BLOCK, BLOCK)]
-            remote(theirs, theirs, e_s.at[6 + side], e_r.at[6 + side], sp=pair).wait_recv()
+            remote(theirs, theirs, e_s[6 + side], e_r.at[6 + side], sp=pair).wait_recv()
     with jax.named_scope("state"):
         state_part(late)
     pump(len(queue))
@@ -827,7 +837,7 @@
     with jax.named_scope("mix_a"):
         for side in range(2):
             theirs = act_a.at[1 - par, :, pl.ds(side * narrow, narrow)]
-            remote(theirs, theirs, e_s.at[4 + side], e_r.at[4 + side], sp=pair).wait_recv()
+            remote(theirs, theirs, e_s[4 + side], e_r.at[4 + side], sp=pair).wait_recv()
 
     def target(who, i):
         first_column = lax.rem(who + 2 * (i // 2), n) * cols + (i % 2) * chunk
@@ -850,7 +860,7 @@
     def pass_on(i):
         remote(got.at[i], got.at[i], d_s.at[i], d_r.at[i], tp=other).wait_recv()
         fsend[i] = (pf[i, 1 - par, t] + got[i, 1 - par].astype(f32)).astype(bf)
-        launch(remote(fsend.at[i], target(k, i), e_s.at[i], e_r.at[i], sp=pair))
+        launch(remote(fsend.at[i], target(k, i), e_s[i], e_r.at[i], sp=pair))
         res[i] = (pf[i, par, t] + got[i, par].astype(f32)).astype(bf)
         launch(pltpu.make_async_copy(res.at[i], target(k, i), o_s.at[i]))
 
@@ -868,9 +878,11 @@
     with jax.named_scope("settle"):
         for i in range(4):
             theirs = target(pair, i)
-            remote(theirs, theirs, e_s.at[i], e_r.at[i], sp=pair).wait_recv()
+            remote(theirs, theirs, e_s[i], e_r.at[i], sp=pair).wait_recv()
 
     with jax.named_scope("drain"):
+        for copies in spreads[-4:]:
+            sent.extend(copies)
         for c in sent:
             if c.is_remote:
                 c.wait_send()
@@ -917,8 +929,8 @@
             vm((4, 2, 2, tokens // 2, cols // 2), f32), vm((4, 2, 2, tokens // 2, cols // 2), bf),
             vm((4, 2, tokens // 2, cols // 2), bf), vm((4, tokens // 2, cols // 2), bf),
             vm((4, tokens // 2, cols // 2), bf),
-            dma((15,)), dma((5, 4)), dma((5, 4)), dma((7,)), dma((7,)), dma((5, 4, 3)), dma((5, 4, 3)),
-            dma((5,)), dma((5,)), dma((4,)), dma((4,)), dma((8,)), dma((8,)), dma((4,)),
+            dma((15,)), dma((16,)), dma((16,)), dma((7,)), dma((7,)), dma((4, 3)), dma((16, 3)),
+            dma((5,)), dma((4,)), dma((4,)), dma((8,)), dma((4,)),
         ],
         compiler_params=pltpu.CompilerParams(collective_id=0, has_side_effects=True),
     )(x, gain, ssm, query, key, value, rate, turn, parts, reads, skip, shift, sinks, ows, owa)

time: 49.4 us -> 48.6 us (0.984)
  Pallas kernels: 47.5 us -> 46.7 us
    pallas_call x1, Pallas kernels: 47.5 us -> 46.7 us  [layer(): pl.pallas_call(layer_kernel, out_shape=jax.ShapeDtypeStruct((tokens // 2,...]
where the time goes in v5:
time: 48.6 us; the launch traced here: 48.4 us
  Pallas kernels  46.7 us (96%)
  local copies, waits for them, and re-layouts  1.67 us (3%)
    pallas_call x1, Pallas kernels, layer(): pl.pallas_call(layer_kernel, out_shape=jax.ShapeDtypeStruct((tokens // 2,...  46.7 us
    unnamed x1, local copies, waits for them, and re-layouts  1.67 us

profile of v5, /device:TPU:0, one launch (start us, length us, event | category | flops | bytes accessed | tf_op | source)
XLA Modules:
  0.0 48.4 jit_solution(4094175134065283168)
XLA Ops:
  0.0 46.7 %shard_map.145 = bf16[64,2048]{1,0:T(8,128)(2,1)} custom-call(bf16[128,1024]{1,0:T(8,128)(2,1)} %x_in.1, f32[1,2048]{1,0:T(1,128)} %bitcast.7, bf16[512,512]{1,0:T(8,128)(2,1)} %ssm.1, bf16[512,512]{1,0:T(8,128)(2,1)} %query.1, bf16[512,128]{1,0:T(8,128)(2,1)} %key_in.1, bf16[512,128]{1,0:T(8,128)(2,1)} %value_in.1, f32[32,64]{1,0:T(8,128)} %rate_in.1, ...), custom_call_target="tpu_custom_call" | custom-call | tf_op jit(solution)/shard_map/pallas_call | solution.py:907
  46.7 1.7 %copy.17 = bf16[64,2048]{1,0:T(8,128)(2,1)} copy(bf16[64,2048]{1,0:T(8,128)(2,1)} %shard_map.145) | data formatting | bytes 524288

commit v6 on v5

--- a/solution.py
+++ b/solution.py
@@ -318,7 +318,7 @@
                  parts, reads, skip, shift, sinks, tab, inm, read, lifts, grows, prefix, u_scr, q_scr,
                  kv_scr, y_scr, act_s, act_a, carry_out, carry_in, scale_out, scale_in, total_in, total_q,
                  give_u, give_q, give_kv, got_u, got_q, got_kv, pa, pf, pb, got, fsend, res,
-                 loc, z_s, z_r, p_s, p_r, x_s, x_r, g_r, d_s, d_r, e_r, o_s):
+                 loc, z_s, z_r, p_s, p_r, x_s, x_r, g_r, d_r, e_r):
     f32, bf = jnp.float32, jnp.bfloat16
     k, f, t = lax.axis_index("sp"), lax.axis_index("fs"), lax.axis_index("tp")
     n, n_fs = 4, 4
@@ -484,7 +484,7 @@
     launch_if(slow, state_weights[1:])
     launch_if(slow | jnp.logical_not(at_end), [give_x])
     launch_if(slow, early_keys)
-    sent.extend(state_weights + early_keys + query_weights + out_weights + attend_weights + [give_x])
+    sent.append(give_x)
     pl.when(k == n - 1)(settle_params)
     with jax.named_scope("tables"):
         columns_of = lax.fori_loop(early, 10, tables, columns_of)
@@ -839,6 +839,9 @@
             theirs = act_a.at[1 - par, :, pl.ds(side * narrow, narrow)]
             remote(theirs, theirs, e_s[4 + side], e_r.at[4 + side], sp=pair).wait_recv()
 
+    for c in state_weights + early_keys + query_weights + out_weights + attend_weights:
+        c.wait_send()
+
     def target(who, i):
         first_column = lax.rem(who + 2 * (i // 2), n) * cols + (i % 2) * chunk
         return out.at[:, pl.ds(pl.multiple_of(first_column, 128), chunk)]
@@ -855,14 +858,14 @@
                 block = total[e * tokens + side * size : e * tokens + (side + 1) * size]
                 pf[i, e, side] = block
                 pb[i, side, e] = block.astype(bf)
-        launch(remote(pb.at[i, other], got.at[i], d_s.at[i], d_r.at[i], tp=other))
+        launch(remote(pb.at[i, other], got.at[i], z_s.at[i], d_r.at[i], tp=other))
 
     def pass_on(i):
-        remote(got.at[i], got.at[i], d_s.at[i], d_r.at[i], tp=other).wait_recv()
+        remote(got.at[i], got.at[i], z_s.at[i], d_r.at[i], tp=other).wait_recv()
         fsend[i] = (pf[i, 1 - par, t] + got[i, 1 - par].astype(f32)).astype(bf)
         launch(remote(fsend.at[i], target(k, i), e_s[i], e_r.at[i], sp=pair))
         res[i] = (pf[i, par, t] + got[i, par].astype(f32)).astype(bf)
-        launch(pltpu.make_async_copy(res.at[i], target(k, i), o_s.at[i]))
+        launch(pltpu.make_async_copy(res.at[i], target(k, i), z_s.at[4 + i]))
 
     for i in range(4):
         if i == 2:
@@ -930,7 +933,7 @@
             vm((4, 2, tokens // 2, cols // 2), bf), vm((4, tokens // 2, cols // 2), bf),
             vm((4, tokens // 2, cols // 2), bf),
             dma((15,)), dma((16,)), dma((16,)), dma((7,)), dma((7,)), dma((4, 3)), dma((16, 3)),
-            dma((5,)), dma((4,)), dma((4,)), dma((8,)), dma((4,)),
+            dma((5,)), dma((4,)), dma((8,)),
         ],
         compiler_params=pltpu.CompilerParams(collective_id=0, has_side_effects=True),
     )(x, gain, ssm, query, key, value, rate, turn, parts, reads, skip, shift, sinks, ows, owa)

time: 48.6 us -> 48.5 us (level)
  no operation moved by 1% of the time
where the time goes in v6:
time: 48.5 us; the launch traced here: 48.3 us
  Pallas kernels  46.6 us (96%)
  local copies, waits for them, and re-layouts  1.67 us (3%)
    pallas_call x1, Pallas kernels, layer(): pl.pallas_call(layer_kernel, out_shape=jax.ShapeDtypeStruct((tokens // 2,...  46.6 us
    unnamed x1, local copies, waits for them, and re-layouts  1.67 us

profile of v6, /device:TPU:0, one launch (start us, length us, event | category | flops | bytes accessed | tf_op | source)
XLA Modules:
  0.0 48.3 jit_solution(16983194084885866715)
XLA Ops:
  0.0 46.6 %shard_map.145 = bf16[64,2048]{1,0:T(8,128)(2,1)} custom-call(bf16[128,1024]{1,0:T(8,128)(2,1)} %x_in.1, f32[1,2048]{1,0:T(1,128)} %bitcast.7, bf16[512,512]{1,0:T(8,128)(2,1)} %ssm.1, bf16[512,512]{1,0:T(8,128)(2,1)} %query.1, bf16[512,128]{1,0:T(8,128)(2,1)} %key_in.1, bf16[512,128]{1,0:T(8,128)(2,1)} %value_in.1, f32[32,64]{1,0:T(8,128)} %rate_in.1, ...), custom_call_target="tpu_custom_call" | custom-call | tf_op jit(solution)/shard_map/pallas_call | solution.py:910
  46.7 1.7 %copy.17 = bf16[64,2048]{1,0:T(8,128)(2,1)} copy(bf16[64,2048]{1,0:T(8,128)(2,1)} %shard_map.145) | data formatting | bytes 524288
